TPU v7x, 32 devices: a whole 2x2x4 slice. The times are simulated.
32 devices in a mesh: rep: 2 (over x), fs: 8 (over z, y), tp: 2 (over core).
Axes of the slice: x: 2, y: 2, z: 4, core: 2. Of those that a mesh axis runs over, the one named last changes fastest.
Arguments:
- tokens: bfloat16 [6144, 2048], P(('rep', 'fs'), 'tp'), may hold values from -6 to 6
- mix_gain: float32 [2048], replicated, may hold values from 0.1 to 1.9
- w_u: bfloat16 [2048, 2048], P('fs', 'tp'), may hold values from -0.125 to 0.125
- w_v: bfloat16 [2048, 2048], P('fs', 'tp'), may hold values from -0.125 to 0.125
- norm_gain: float32 [2048], P('tp'), may hold values from 0.1 to 1.9
- mix_weight: bfloat16 [16, 128, 128], P('tp'), may hold values from -0.5 to 0.5
- mix_bias: float32 [16, 128], P('tp'), may hold values from 0.1 to 1.9
- w_mix_out: bfloat16 [2048, 2048], P('tp', 'fs'), may hold values from -0.125 to 0.125
- ffn_gain: float32 [2048], replicated, may hold values from 0.1 to 1.9
- w_gate: bfloat16 [2048, 3072], P('fs', 'tp'), may hold values from -0.125 to 0.125
- w_value: bfloat16 [2048, 3072], P('fs', 'tp'), may hold values from -0.125 to 0.125
- taps_gate: bfloat16 [3, 3072], P(None, 'tp'), may hold values from -3.5 to 3.5
- taps_value: bfloat16 [3, 3072], P(None, 'tp'), may hold values from -3.5 to 3.5
- w_down: bfloat16 [3072, 2048], P('tp', 'fs'), may hold values from -0.109375 to 0.109375
Outputs:
- layer_out: bfloat16 [6144, 2048], P(('rep', 'fs'), 'tp')
All inputs are finite; a program needn't handle non-finite values.
Results may differ from a plain program's by a relative error of at most 0.017.
Values may be sent and summed in bfloat16 or wider, within the bound.
A program may use at most 64 MiB of HBM per device.

v0:
```python
import functools

import jax
import jax.numpy as jnp
from jax import lax
from jax.experimental import pallas as pl
from jax.experimental.pallas import tpu as pltpu
from jax.sharding import PartitionSpec as P

EPS_RMS = 1e-06
EPS_LN = 1e-05
F32 = jnp.float32
BF16 = jnp.bfloat16
MESH = pl.DeviceIdType.MESH


def own_half(array, axis):
    share = array.shape[axis] // lax.axis_size("rep")
    return lax.dynamic_slice_in_dim(array, lax.axis_index("rep") * share, share, axis)


def layer_kernel(
    n, nr, nt,
    tok, mix_gain, w_in, norm_gain, mixw, bias, w_out, ffn_gain, w_up, taps_g, taps_v, w_dn,
    out,
    g_in, g_out, g_up, g_dn, feat, feat2, normed, uv, hidden, gv, act, part1, part2, got1, got2,
    w_send, w_recv, w_local, f_send, f_recv, p_send, p_recv,
):
    rep, fs, tp = lax.axis_index("rep"), lax.axis_index("fs"), lax.axis_index("tp")
    seq, own_width = tok.shape
    nz = n // 2
    z, y = fs // 2, fs % 2
    per = n // nt
    depth = normed.shape[2]
    mine = (w_in, w_out, w_up, w_dn)
    gathered = (g_in, g_out, g_up, g_dn)
    offsets = [(a, b) for a in range(nr) for b in range(nt) if (a, b) != (0, 0)]

    def peer(a, b):
        return {"rep": lax.rem(rep + a, nr), "tp": lax.rem(tp + b, nt)}

    barrier = pltpu.get_barrier_semaphore()
    line = (lax.rem(z + 1, nz), lax.rem(z + nz - 1, nz))
    greeted = [{"fs": z * 2 + 1 - y}] + [{"fs": at * 2 + y} for at in line]
    greeted += [peer(a, b) for a, b in offsets]
    for target in greeted:
        pl.semaphore_signal(barrier, inc=1, device_id=target, device_id_type=MESH)
    pl.semaphore_wait(barrier, len(greeted))

    def hop(stage, block, way):
        target = (fs + 2, fs - 2, z * 2 + 1 - y)[way]
        return pltpu.make_async_remote_copy(
            src_ref=gathered[stage].at[block],
            dst_ref=gathered[stage].at[block],
            send_sem=w_send.at[stage, way, block],
            recv_sem=w_recv.at[stage, block],
            device_id={"fs": target},
            device_id_type=MESH,
        )

    def ways(src):
        return (
            jnp.logical_and(src <= z, z < nz - 1),
            jnp.logical_and(src >= z, z > 0),
        )

    def forward(stage, src):
        block = src * 2 + y
        hop(stage, block, 2).start()
        for way, used in enumerate(ways(src)):
            @pl.when(used)
            def _():
                hop(stage, block, way).start()

    def arrived(stage, block):
        hop(stage, block, 2).wait_recv()

    def order(i):
        near = jnp.minimum(z, nz - 1 - z)
        swing = z + ((i + 1) // 2) * (1 - 2 * (i % 2))
        rest = jnp.where(z < nz - 1 - z, i, nz - 1 - i)
        return jnp.where(i <= 2 * near, swing, rest)

    def stage_loop(stage, compute, begin, middle):
        def step(i, _):
            src = order(i)

            @pl.when(i > 0)
            def _():
                arrived(stage, src * 2 + y)
                forward(stage, src)

            compute(src * 2 + y)

            @pl.when(i > 0)
            def _():
                other = order(i - 1) * 2 + 1 - y
                arrived(stage, other)
                compute(other)

            return 0

        lax.fori_loop(begin, nz, step, 0)
        middle()
        last = order(nz - 1) * 2 + 1 - y
        arrived(stage, last)
        compute(last)

    locals_ = [
        pltpu.make_async_copy(mine[k], gathered[k].at[fs], w_local.at[k]) for k in range(4)
    ]
    own_tok = pltpu.make_async_copy(tok, feat.at[rep, tp], w_local.at[4])
    for copy in locals_ + [own_tok]:
        copy.start()

    def share(turn, slabs):
        copies = []
        for k, (a, b) in enumerate(offsets):
            copies.append(
                pltpu.make_async_remote_copy(
                    src_ref=slabs.at[rep, tp],
                    dst_ref=slabs.at[rep, tp],
                    send_sem=f_send.at[turn, k],
                    recv_sem=f_recv.at[turn, k],
                    device_id=peer(a, b),
                    device_id_type=MESH,
                )
            )
        return copies

    def share_wait(turn, slabs):
        for k, (a, b) in enumerate(offsets):
            slab = slabs.at[lax.rem(rep + nr - a, nr), lax.rem(tp + nt - b, nt)]
            pltpu.make_async_remote_copy(
                src_ref=slab, dst_ref=slab, send_sem=f_send.at[turn, k],
                recv_sem=f_recv.at[turn, k], device_id=peer(a, b), device_id_type=MESH,
            ).wait_recv()

    def norm(slabs, gain):
        for r in range(nr):
            total = jnp.zeros((seq, 1), F32)
            for t in range(nt):
                values = slabs[r, t].astype(F32)
                total += jnp.sum(values * values, axis=1, keepdims=True)
            scale = lax.rsqrt(total / (nt * own_width) + EPS_RMS)
            for t in range(nt):
                for j in range(per):
                    values = slabs[r, t, :, j * depth : (j + 1) * depth].astype(F32)
                    normed[t * per + j, r * seq : (r + 1) * seq, :] = (
                        values * scale * gain[t * per + j]
                    ).astype(BF16)

    def piece(turn, part, got, block, r):
        return pltpu.make_async_remote_copy(
            src_ref=part.at[block, r],
            dst_ref=got.at[rep * nt + tp, block % per],
            send_sem=p_send.at[turn, block, r],
            recv_sem=p_recv.at[turn, rep * nt + tp, block % per],
            device_id={"rep": r, "tp": block // per},
            device_id_type=MESH,
        )

    def abroad(block, r):
        return jnp.logical_or(block // per != tp, r != rep)

    def project(turn, left, gathered_w, part, got, block):
        for r in range(nr):
            part[block, r] = jnp.dot(
                left[r], gathered_w[block], preferred_element_type=F32
            ).astype(BF16)

            @pl.when(abroad(block, r))
            def _():
                piece(turn, part, got, block, r).start()

    def collect(turn, part, got, base, emit):
        for j in range(per):
            total = part[tp * per + j, rep].astype(F32)
            for a, b in offsets:
                slot = lax.rem(rep + a, nr) * nt + lax.rem(tp + b, nt)
                landing = got.at[slot, j]
                pltpu.make_async_remote_copy(
                    src_ref=landing, dst_ref=landing, send_sem=p_send.at[turn, 0, 0],
                    recv_sem=p_recv.at[turn, slot, j], device_id=peer(a, b),
                    device_id_type=MESH,
                ).wait_recv()
                total += got[slot, j].astype(F32)
            width = total.shape[1]
            span = slice(j * width, (j + 1) * width)
            emit(span, (base(span).astype(F32) + total).astype(BF16))

    for copy in locals_ + [own_tok]:
        copy.wait()
    for copy in share(0, feat):
        copy.start()
    forward(0, z)
    forward(1, z)
    forward(2, z)
    uv[...] = jnp.zeros_like(uv)
    gv[...] = jnp.zeros_like(gv)
    share_wait(0, feat)
    norm(feat, mix_gain)

    def in_block(block):
        for r in range(nr):
            rows = slice(r * seq, (r + 1) * seq)
            uv[rows, :] += jnp.dot(
                normed[block, rows, :], g_in[block], preferred_element_type=F32
            )

    stage_loop(0, in_block, 0, lambda: forward(3, z))

    groups, block_len = mixw.shape[0], mixw.shape[1]
    group_width = uv.shape[1] // 2 // groups

    for r in range(nr):
        def mix_rows(i, _):
            start = pl.multiple_of(i * block_len, block_len)
            rows = pl.ds(pl.multiple_of(r * seq + i * block_len, block_len), block_len)
            for g in range(groups):
                at = g * group_width
                half = groups * group_width
                activated = jax.nn.gelu(uv[rows, half + at : half + at + group_width])
                centred = activated - jnp.mean(activated, axis=1, keepdims=True)
                spread = jnp.mean(centred * centred, axis=1, keepdims=True)
                v_norm = (
                    centred * lax.rsqrt(spread + EPS_LN) * norm_gain[:, at : at + group_width]
                ).astype(BF16)
                mixed = jnp.dot(mixw[g], v_norm, preferred_element_type=F32) + bias[g]
                hidden[r, pl.ds(start, block_len), at : at + group_width] = (
                    jax.nn.gelu(uv[rows, at : at + group_width]) * mixed
                ).astype(BF16)
            return 0

        lax.fori_loop(0, seq // block_len, mix_rows, 0)

    stage_loop(
        1, functools.partial(project, 0, hidden, g_out, part1, got1), 0, lambda: None
    )

    def relay(stage, begin, end):
        def step(i, _):
            arrived(stage, order(i) * 2 + y)
            forward(stage, order(i))
            return 0

        lax.fori_loop(begin, end, step, 0)

    def put_middle(span, value):
        feat2[rep, tp, :, span] = value

    relay(2, 1, nz // 2)
    collect(0, part1, got1, lambda span: tok[:, span], put_middle)
    for copy in share(1, feat2):
        copy.start()
    relay(2, nz // 2, nz)
    share_wait(1, feat2)
    norm(feat2, ffn_gain)

    def up_block(block):
        for r in range(nr):
            gv[r, 8:, :] += jnp.dot(
                normed[block, r * seq : (r + 1) * seq, :],
                g_up[block],
                preferred_element_type=F32,
            )

    def up_step(i, _):
        up_block(order(i) * 2 + y)

        @pl.when(i > 0)
        def _():
            arrived(3, order(i) * 2 + y)
            forward(3, order(i))

        other = order(i) * 2 + 1 - y
        arrived(2, other)
        up_block(other)
        return 0

    lax.fori_loop(0, nz, up_step, 0)

    units = act.shape[2]
    taps_len = taps_g.shape[0]
    chunk = 128 if units % 128 == 0 else units
    for r in range(nr):
        for at in range(0, units, chunk):
            gate = jnp.zeros((seq, chunk), F32)
            value = jnp.zeros((seq, chunk), F32)
            for k in range(taps_len):
                first = 8 - (taps_len - 1) + k
                gate += taps_g[k : k + 1, at : at + chunk] * gv[r, first : first + seq, at : at + chunk]
                value += (
                    taps_v[k : k + 1, at : at + chunk]
                    * gv[r, first : first + seq, units + at : units + at + chunk]
                )
            act[r, :, at : at + chunk] = (jax.nn.gelu(gate) * value).astype(BF16)

    down = functools.partial(project, 1, act, g_dn, part2, got2)

    def down_own(i, _):
        down(order(i) * 2 + y)
        return 0

    def down_other(i, _):
        arrived(3, order(i) * 2 + 1 - y)
        down(order(i) * 2 + 1 - y)
        return 0

    lax.fori_loop(0, nz, down_own, 0)
    lax.fori_loop(0, nz, down_other, 0)

    def put_out(span, value):
        out[:, span] = value

    collect(1, part2, got2, lambda span: feat2[rep, tp, :, span], put_out)

    for turn, slabs in enumerate((feat, feat2)):
        for copy in share(turn, slabs):
            copy.wait_send()

    def drain_pieces(block, _):
        for r in range(nr):
            @pl.when(abroad(block, r))
            def _():
                piece(0, part1, got1, block, r).wait_send()
                piece(1, part2, got2, block, r).wait_send()
        return 0

    lax.fori_loop(0, n, drain_pieces, 0)

    def drain_hops(src, _):
        for stage in range(4):
            hop(stage, src * 2 + y, 2).wait_send()
            for way, used in enumerate(ways(src)):
                @pl.when(used)
                def _():
                    hop(stage, src * 2 + y, way).wait_send()
        return 0

    lax.fori_loop(0, nz, drain_hops, 0)


def on_device(
    tokens,
    mix_gain,
    w_u,
    w_v,
    norm_gain,
    mix_weight,
    mix_bias,
    w_mix_out,
    ffn_gain,
    w_gate,
    w_value,
    taps_gate,
    taps_value,
    w_down,
):
    n, nr, nt = lax.axis_size("fs"), lax.axis_size("rep"), lax.axis_size("tp")
    seq, own_width = tokens.shape
    depth, per = own_width * nt // n, n // nt
    block_len = mix_weight.shape[1]
    lower_mask = jnp.arange(block_len)[:, None] >= jnp.arange(block_len)[None, :]
    mixw = own_half(mix_weight, 0)
    mixw = jnp.where(lower_mask[None], mixw, jnp.zeros_like(mixw))
    w_in = jnp.concatenate((own_half(w_u, 1), own_half(w_v, 1)), 1)
    w_up = jnp.concatenate((own_half(w_gate, 1), own_half(w_value, 1)), 1)
    w_out, w_dn = own_half(w_mix_out, 0), own_half(w_down, 0)
    operands = (
        tokens,
        mix_gain.reshape(n, 1, depth),
        w_in,
        own_half(norm_gain, 0)[None, :],
        mixw,
        own_half(mix_bias, 0)[:, :, None],
        w_out,
        ffn_gain.reshape(n, 1, depth),
        w_up,
        own_half(taps_gate, 1).astype(F32),
        own_half(taps_value, 1).astype(F32),
        w_dn,
    )
    vmem, sem = pltpu.VMEM, pltpu.SemaphoreType.DMA
    others = nr * nt - 1
    return pl.pallas_call(
        functools.partial(layer_kernel, n, nr, nt),
        out_shape=jax.ShapeDtypeStruct((seq, own_width), BF16),
        in_specs=[pl.BlockSpec(memory_space=vmem)] * len(operands),
        out_specs=pl.BlockSpec(memory_space=vmem),
        scratch_shapes=[
            vmem((n,) + w_in.shape, BF16),
            vmem((n,) + w_out.shape, BF16),
            vmem((n,) + w_up.shape, BF16),
            vmem((n,) + w_dn.shape, BF16),
            vmem((nr, nt, seq, own_width), BF16),
            vmem((nr, nt, seq, own_width), BF16),
            vmem((n, nr * seq, depth), BF16),
            vmem((nr * seq, w_in.shape[1]), F32),
            vmem((nr, seq, w_out.shape[0]), BF16),
            vmem((nr, seq + 8, w_up.shape[1]), F32),
            vmem((nr, seq, w_dn.shape[0]), BF16),
            vmem((n, nr, seq, depth), BF16),
            vmem((n, nr, seq, depth), BF16),
            vmem((nr * nt, per, seq, depth), BF16),
            vmem((nr * nt, per, seq, depth), BF16),
            sem((4, 3, n)),
            sem((4, n)),
            sem((5,)),
            sem((2, others)),
            sem((2, others)),
            sem((2, n, nr)),
            sem((2, nr * nt, per)),
        ],
        compiler_params=pltpu.CompilerParams(
            collective_id=0, has_side_effects=True, vmem_limit_bytes=67043328
        ),
    )(*operands)


def solution(mesh):
    placed = (
        P(("rep", "fs"), "tp"),
        P(),
        P("fs", "tp"),
        P("fs", "tp"),
        P("tp"),
        P("tp", None, None),
        P("tp", None),
        P("tp", "fs"),
        P(),
        P("fs", "tp"),
        P("fs", "tp"),
        P(None, "tp"),
        P(None, "tp"),
        P("tp", "fs"),
    )
    return jax.shard_map(
        on_device, mesh=mesh, in_specs=placed, out_specs=P(("rep", "fs"), "tp"), check_vma=False
    )
```

profile of v0, /device:TPU:1, one launch (start us, length us, event | category | flops | bytes accessed | tf_op | source)
XLA Modules:
  0.0 228.0 jit_solution(5411179548255535654)
XLA Ops:
  0.0 0.0 copy-start
  0.0 1.4 dynamic_slice.35
  1.4 0.7 fusion
  2.1 1.3 dynamic-slice_convert_fusion
  3.4 1.6 dynamic-slice_select_fusion.mixw
  5.0 0.0 copy-start.3
  5.0 0.0 copy-start.4
  5.0 0.9 copy.15.bias
  5.9 1.7 constant_dynamic-slice_fusion.3.w_out
  7.5 0.0 copy-done
  7.6 0.8 constant_dynamic-slice_fusion.w_dn
  8.3 0.0 copy-done.3
  8.3 0.0 copy-done.4
  8.3 0.0 copy-start.2
  8.4 0.0 copy-start.1
  8.4 0.9 pad_maximum_fusion.1.w_in
  9.3 0.4 copy-done.2
  9.7 0.2 copy-done.1
  9.9 0.1 constant_dynamic-slice_fusion.1
  10.0 0.9 pad_maximum_fusion.w_up
  10.9 215.0 %shard_map.136 = bf16[384,1024]{1,0:T(8,128)(2,1)} custom-call(bf16[384,1024]{1,0:T(8,128)(2,1)} %tok.1, f32[8,1,256]{2,1,0:T(1,128)} %bitcast.6, bf16[256,1024]{1,0:T(8,128)(2,1)} %pad_maximum_fusion.1.w_in, f32[1,512]{1,0:T(1,128)} %bitcast.5, bf16[4,128,128]{2,1,0:T(8,128)(2,1)} %dynamic-slice_select_fusion.mixw, f32[4,128,1]{2,1,0:T(8,128)} %copy.15.bias, ...), custom_call_target="tpu_custom_call" | custom-call | tf_op jit(solution)/shard_map/pallas_call | solution.py:386
  225.9 2.1 copy.17
  (2 shorter events, 0.1 us)
Async XLA Ops:
  0.0 7.6 %copy-start = (bf16[1536,256]{1,0:T(8,128)(2,1)S(1)}, bf16[1536,256]{1,0:T(8,128)(2,1)}, u32[]{:S(2)}) copy-start(bf16[1536,256]{1,0:T(8,128)(2,1)} %param.27) | copy-start | bytes 2359300
  5.0 3.4 %copy-start.3 = (bf16[256,1024]{1,0:T(8,128)(2,1)S(1)}, bf16[256,1024]{1,0:T(8,128)(2,1)}, u32[]{:S(2)}) copy-start(bf16[256,1024]{1,0:T(8,128)(2,1)} %param.17) | copy-start | bytes 1572868
  5.0 3.4 %copy-start.4 = (bf16[256,1024]{1,0:T(8,128)(2,1)S(1)}, bf16[256,1024]{1,0:T(8,128)(2,1)}, u32[]{:S(2)}) copy-start(bf16[256,1024]{1,0:T(8,128)(2,1)} %param.16) | copy-start | bytes 1572868
  8.3 1.3 copy-start.2
  8.4 1.5 copy-start.1
where the time goes:
time: 228 us
  Pallas kernels  215 us (94%)
  local copies, waits for them, and re-layouts  8.26 us (4%)
  other arithmetic  4.69 us (2%)
    pallas_call x1, Pallas kernels, on_device(): pl.pallas_call(functools.partial(layer_kernel, n, nr, nt), out_shape=jax....  215 us

commit v1 on v0

--- a/solution.py
+++ b/solution.py
@@ -418,6 +418,690 @@
     )(*operands)
 
 
+def plane_kernel(
+    n, nr, nt,
+    tok, mix_gain, w_u, w_v, norm_gain, mixw, bias, w_out, ffn_gain, w_gate, w_value, taps_g, taps_v, w_dn,
+    out,
+    g_in, g_out, g_up, g_dn, feat, feat2, mid, normed, uv, hidden, gv, act,
+    part1, part2, inc1, inc2, got1, got2, raw_mix, mix_low, gain_v, bias_all, bias_col, tg, tv,
+    l_sem, y_send, y_recv, z_send, z_recv, d_send, d_recv, s_local, s_send, s_recv,
+    a_send, a_recv, f_send, r_send, i_recv, t_recv,
+):
+    rep, fs, tp = lax.axis_index("rep"), lax.axis_index("fs"), lax.axis_index("tp")
+    seq, own_width = tok.shape
+    ny, nz = 2, n // 2
+    z, y = fs // ny, fs % ny
+    per = n // nt
+    width = own_width // per
+    quarter = rep * ny + y
+    other_quarter = rep * ny + 1 - y
+    fs_y = z * ny + 1 - y
+    home = rep == tp
+    away = rep != tp
+    cu, cf = g_out.shape[2], g_dn.shape[2]
+    mid_rows = (tok, mid)
+    feats = (feat, feat2)
+
+    barrier = pltpu.get_barrier_semaphore()
+    greeted = [{"tp": 1 - tp}]
+    greeted += [{"rep": 1 - rep, "tp": t} for t in range(nt)]
+    greeted += [{"fs": fs_y, "tp": t} for t in range(nt)]
+    greeted += [{"fs": lax.rem(z + k, nz) * ny + y} for k in range(1, nz)]
+
+    def item(k, block, half):
+        if k == 0:
+            return g_in.at[half, block]
+        if k == 1:
+            return g_out.at[block, half]
+        if k == 2:
+            return g_up.at[half, block]
+        return g_dn.at[block, half]
+
+    def pieces(k, which, block):
+        whole = item(k, block, tp)
+        if k in (0, 2):
+            first, second, size = (w_u, w_v, cu) if k == 0 else (w_gate, w_value, cf)
+            cols = pl.ds(pl.multiple_of(which * size, 128), size)
+            return (
+                (first.at[:, cols], whole.at[:, pl.ds(0, size)]),
+                (second.at[:, cols], whole.at[:, pl.ds(size, size)]),
+            )
+        source, size = (w_out, cu) if k == 1 else (w_dn, cf)
+        rows = pl.ds(pl.multiple_of(which * size, 128), size)
+        return ((source.at[rows, :], whole),)
+
+    def own_load(k):
+        return [
+            pltpu.make_async_copy(src, dst, l_sem.at[k, i])
+            for i, (src, dst) in enumerate(pieces(k, quarter, fs))
+        ]
+
+    def across(k, block):
+        return [
+            pltpu.make_async_remote_copy(
+                src_ref=src, dst_ref=dst, send_sem=y_send.at[k, i], recv_sem=y_recv.at[k, i],
+                device_id={"fs": fs_y}, device_id_type=MESH,
+            )
+            for i, (src, dst) in enumerate(pieces(k, other_quarter, block))
+        ]
+
+    def z_copy(k, block, step):
+        return pltpu.make_async_remote_copy(
+            src_ref=item(k, block, tp), dst_ref=item(k, block, tp),
+            send_sem=z_send.at[k, block, step + 2], recv_sem=z_recv.at[k, block],
+            device_id={"fs": fs + ny * step}, device_id_type=MESH,
+        )
+
+    def d_copy(k, block):
+        return pltpu.make_async_remote_copy(
+            src_ref=item(k, block, tp), dst_ref=item(k, block, tp),
+            send_sem=d_send.at[k, block], recv_sem=d_recv.at[k, block],
+            device_id={"tp": 1 - tp}, device_id_type=MESH,
+        )
+
+    def inside(step):
+        return jnp.logical_and(z + step >= 0, z + step < nz)
+
+    def spread(k, block):
+        for step in (2, -2, 1, -1):
+            @pl.when(inside(step))
+            def _():
+                z_copy(k, block, step).start()
+        d_copy(k, block).start()
+
+    def arrive(k, block):
+        landing = item(k, block, tp)
+        pltpu.make_async_remote_copy(
+            src_ref=landing, dst_ref=landing, send_sem=z_send.at[k, block, 2],
+            recv_sem=z_recv.at[k, block], device_id={"tp": 1 - tp}, device_id_type=MESH,
+        ).wait_recv()
+        d_copy(k, block).start()
+
+    def cross_over(k):
+        for copy in across(k, fs_y):
+            copy.wait_recv()
+        spread(k, fs_y)
+
+    def relays():
+        return [
+            (sign, z - sign * far, jnp.logical_and(inside(sign), inside(-sign * far)))
+            for sign in (1, -1)
+            for far in range(2, nz)
+        ]
+
+    def relay(k):
+        for at in range(ny):
+            for sign, source, used in relays():
+                @pl.when(used)
+                def _():
+                    arrive(k, source * ny + at)
+                    z_copy(k, source * ny + at, sign).start()
+
+    def relayed(source):
+        up = jnp.logical_and(z - source >= 2, inside(1))
+        down = jnp.logical_and(source - z >= 2, inside(-1))
+        return jnp.logical_or(up, down)
+
+    def need(k, block):
+        source = block // ny
+        @pl.when(jnp.logical_and(source != z, jnp.logical_not(relayed(source))))
+        def _():
+            arrive(k, block)
+
+    def partner_wait(k, block):
+        landing = item(k, block, 1 - tp)
+        pltpu.make_async_remote_copy(
+            src_ref=landing, dst_ref=landing, send_sem=d_send.at[k, block],
+            recv_sem=d_recv.at[k, block], device_id={"tp": 1 - tp}, device_id_type=MESH,
+        ).wait_recv()
+
+    def order(i):
+        near = jnp.minimum(z, nz - 1 - z)
+        swing = z + ((i + 1) // 2) * (1 - 2 * (i % 2))
+        rest = jnp.where(z < nz - 1 - z, i, nz - 1 - i)
+        return jnp.where(i <= 2 * near, swing, rest)
+
+    def near_block(i):
+        return order(i // ny) * ny + lax.rem(y + i, ny)
+
+    def plain_block(i):
+        return order(i // ny) * ny + lax.rem(i, ny)
+
+    small = [
+        (mixw.at[pl.ds(quarter * raw_mix.shape[1], raw_mix.shape[1])], raw_mix.at[tp]),
+        (norm_gain.at[:, pl.ds(pl.multiple_of(quarter * cu, 128), cu)], gain_v.at[tp]),
+        (bias, bias_all.at[tp]),
+        (taps_g.at[:, pl.ds(pl.multiple_of(quarter * cf, 128), cf)], tg.at[tp]),
+        (taps_v.at[:, pl.ds(pl.multiple_of(quarter * cf, 128), cf)], tv.at[tp]),
+    ]
+    small_local = [
+        pltpu.make_async_copy(src, dst, s_local.at[i]) for i, (src, dst) in enumerate(small)
+    ]
+    small_away = [
+        pltpu.make_async_remote_copy(
+            src_ref=src, dst_ref=dst, send_sem=s_send.at[i], recv_sem=s_recv.at[i],
+            device_id={"tp": 1 - tp}, device_id_type=MESH,
+        )
+        for i, (src, dst) in enumerate(small)
+    ]
+
+    def ag_source(turn, i):
+        if turn == 0:
+            return tok.at[:, pl.ds(pl.multiple_of(i * width, 128), width)]
+        return mid.at[i]
+
+    def ag_copy(turn, i, way):
+        block = tp * per + i
+        device = ({"rep": 1 - rep, "tp": rep}, {"fs": fs_y, "tp": rep}, {"tp": 1 - tp})[way]
+        return pltpu.make_async_remote_copy(
+            src_ref=ag_source(turn, i), dst_ref=feats[turn].at[y, block],
+            send_sem=a_send.at[turn, way, i], recv_sem=a_recv.at[turn, y, block],
+            device_id=device, device_id_type=MESH,
+        )
+
+    def ag_send(turn, i):
+        ag_copy(turn, i, 0).start()
+        ag_copy(turn, i, 1).start()
+
+        @pl.when(away)
+        def _():
+            ag_copy(turn, i, 2).start()
+
+        @pl.when(home)
+        def _():
+            feats[turn][y, tp * per + i] = ag_source(turn, i)[...]
+
+    def ag_pass(turn, i):
+        slot = jnp.where(home, 1 - y, y)
+        block = jnp.where(home, (nt - 1) * per, 0) + i
+        return pltpu.make_async_remote_copy(
+            src_ref=feats[turn].at[slot, block], dst_ref=feats[turn].at[slot, block],
+            send_sem=f_send.at[turn, i], recv_sem=a_recv.at[turn, slot, block],
+            device_id={
+                "rep": jnp.where(home, 1 - rep, rep),
+                "fs": jnp.where(home, fs, fs_y),
+            },
+            device_id_type=MESH,
+        )
+
+    def ag_landed(turn, slot, block):
+        landing = feats[turn].at[slot, block]
+        pltpu.make_async_remote_copy(
+            src_ref=landing, dst_ref=landing, send_sem=f_send.at[turn, 0],
+            recv_sem=a_recv.at[turn, slot, block], device_id={"tp": 1 - tp}, device_id_type=MESH,
+        ).wait_recv()
+
+    def ag_forward(turn):
+        def step(i, _):
+            slot = jnp.where(home, 1 - y, y)
+            ag_landed(turn, slot, jnp.where(home, (nt - 1) * per, 0) + i)
+            ag_pass(turn, i).start()
+            return 0
+
+        lax.fori_loop(0, per, step, 0)
+
+    def ag_wait(turn, slot):
+        def step(block, _):
+            half = block // per
+            local = jnp.logical_and(home, jnp.logical_and(slot == y, half == tp))
+            passed_home = jnp.logical_and(home, jnp.logical_and(slot != y, half == nt - 1))
+            passed_away = jnp.logical_and(away, jnp.logical_and(slot == y, half == 0))
+            done = jnp.logical_or(local, jnp.logical_or(passed_home, passed_away))
+
+            @pl.when(jnp.logical_not(done))
+            def _():
+                ag_landed(turn, slot, block)
+
+            return 0
+
+        lax.fori_loop(0, n, step, 0)
+
+    def norm(turn, slot, gain):
+        slabs = feats[turn]
+
+        def add(block, total):
+            values = slabs[slot, block].astype(F32)
+            return total + jnp.sum(values * values, axis=1, keepdims=True)
+
+        total = lax.fori_loop(0, n, add, jnp.zeros((seq, 1), F32))
+        scale = lax.rsqrt(total / (n * width) + EPS_RMS)
+
+        def put(block, _):
+            values = slabs[slot, block].astype(F32)
+            cols = pl.ds(pl.multiple_of(block * width, 128), width)
+            normed[block, slot] = (values * scale * gain[:, cols]).astype(BF16)
+            return 0
+
+        lax.fori_loop(0, n, put, 0)
+
+    def gathered_loop(k, multiply):
+        def step(i, _):
+            block = near_block(i)
+            need(k, block)
+            multiply(block, tp)
+
+            @pl.when(i > 0)
+            def _():
+                before = near_block(i - 1)
+                partner_wait(k, before)
+                multiply(before, 1 - tp)
+
+            return 0
+
+        lax.fori_loop(0, n, step, 0)
+        last = near_block(n - 1)
+        partner_wait(k, last)
+        multiply(last, 1 - tp)
+
+    def even(block):
+        return lax.rem(block, 2) == 0
+
+    def both(*conditions):
+        return functools.reduce(jnp.logical_and, conditions)
+
+    parts, incs, gots = (part1, part2), (inc1, inc2), (got1, got2)
+
+    def r_copy(turn, r, block, kind):
+        slot = lax.rem(y + r, 2)
+        core, at = block // per, lax.rem(block, per)
+        got, inc = gots[turn], incs[turn]
+        dst, sem, device = {
+            "diag_x": (inc.at[block], i_recv.at[turn, block], {"rep": 1 - rep}),
+            "diag_y": (inc.at[block], i_recv.at[turn, block], {"fs": fs_y}),
+            "pair": (got.at[0, at], t_recv.at[turn, 0, at], {"tp": 1 - tp}),
+            "x": (got.at[1, at], t_recv.at[turn, 1, at], {"rep": 1 - rep, "tp": core}),
+            "y": (got.at[2, at], t_recv.at[turn, 2, at], {"fs": fs_y, "tp": core}),
+        }[kind]
+        return pltpu.make_async_remote_copy(
+            src_ref=parts[turn].at[slot, block], dst_ref=dst, send_sem=r_send.at[turn, r, block],
+            recv_sem=sem, device_id=device, device_id_type=MESH,
+        )
+
+    def cases(block):
+        return (
+            (1, "diag_x", both(away, even(block)), True),
+            (1, "diag_y", both(away, jnp.logical_not(even(block))), True),
+            (1, "y", both(home, jnp.logical_not(even(block))), True),
+            (0, "pair", both(home, block // per != tp), True),
+            (0, "x", both(away, even(block)), True),
+            (1, "y", both(home, even(block)), False),
+            (0, "x", both(away, jnp.logical_not(even(block))), False),
+        )
+
+    def project(turn, left, weight, block):
+        size = weight.shape[1] * weight.shape[2]
+        right = weight[block].reshape(size, weight.shape[3])
+        for r in (1, 0):
+            slot = lax.rem(y + r, 2)
+            parts[turn][slot, block] = jnp.dot(
+                left[slot], right, preferred_element_type=F32
+            ).astype(BF16)
+            for row, kind, used, now in cases(block):
+                if row == r and now:
+                    @pl.when(used)
+                    def _():
+                        r_copy(turn, r, block, kind).start()
+
+        @pl.when(both(home, block // per == tp))
+        def _():
+            gots[turn][0, lax.rem(block, per)] = parts[turn][y, block]
+
+    def join(turn, block):
+        for r, kind, used, now in cases(block):
+            if not now:
+                @pl.when(used)
+                def _():
+                    landing = incs[turn].at[block]
+                    pltpu.make_async_remote_copy(
+                        src_ref=landing, dst_ref=landing, send_sem=r_send.at[turn, 0, 0],
+                        recv_sem=i_recv.at[turn, block], device_id={"rep": 1 - rep},
+                        device_id_type=MESH,
+                    ).wait_recv()
+                    slot = lax.rem(y + r, 2)
+                    parts[turn][slot, block] = (
+                        parts[turn][slot, block].astype(F32) + incs[turn][block].astype(F32)
+                    ).astype(BF16)
+                    r_copy(turn, r, block, kind).start()
+
+    def landed(turn, kind, at):
+        landing = gots[turn].at[kind, at]
+        pltpu.make_async_remote_copy(
+            src_ref=landing, dst_ref=landing, send_sem=r_send.at[turn, 0, 0],
+            recv_sem=t_recv.at[turn, kind, at], device_id={"rep": 1 - rep}, device_id_type=MESH,
+        ).wait_recv()
+
+    def collect(turn, block):
+        at = lax.rem(block, per)
+
+        @pl.when(away)
+        def _():
+            landed(turn, 0, at)
+
+        landed(turn, 1, at)
+        landed(turn, 2, at)
+        got = gots[turn]
+        total = got[0, at].astype(F32) + got[1, at].astype(F32) + got[2, at].astype(F32)
+        cols = pl.ds(pl.multiple_of(at * width, 128), width)
+        if turn == 0:
+            mid[at] = (tok[:, cols].astype(F32) + total).astype(BF16)
+            ag_send(1, at)
+        else:
+            out[:, cols] = (mid[at].astype(F32) + total).astype(BF16)
+
+    def scatter_loop(k, turn, left, weight):
+        def step(i, _):
+            @pl.when(i < n)
+            def _():
+                need(k, plain_block(i))
+
+            @pl.when(both(i >= 1, i < n + 1))
+            def _():
+                block = plain_block(i - 1)
+                partner_wait(k, block)
+                project(turn, left, weight, block)
+
+            @pl.when(both(i >= 3, i < n + 3))
+            def _():
+                join(turn, plain_block(i - 3))
+
+            @pl.when(i >= 5)
+            def _():
+                block = plain_block(i - 5)
+
+                @pl.when(block // per == tp)
+                def _():
+                    collect(turn, block)
+
+            return 0
+
+        lax.fori_loop(0, n + 5, step, 0)
+
+    for k in range(4):
+        for copy in own_load(k):
+            copy.start()
+    for copy in small_local:
+        copy.start()
+    for target in greeted:
+        pl.semaphore_signal(barrier, inc=1, device_id=target, device_id_type=MESH)
+    pl.semaphore_wait(barrier, len(greeted))
+
+    for copy in across(0, fs):
+        copy.start()
+    for i in range(per):
+        ag_send(0, i)
+    for k in range(2):
+        for copy in own_load(k):
+            copy.wait()
+        spread(k, fs)
+    for copy in across(1, fs) + small_away:
+        copy.start()
+    cross_over(0)
+    for k in (2, 3):
+        for copy in own_load(k):
+            copy.wait()
+    ag_forward(0)
+    cross_over(1)
+    for k in (2, 3):
+        for copy in across(k, fs):
+            copy.start()
+    uv[...] = jnp.zeros_like(uv)
+    gv[...] = jnp.zeros_like(gv)
+    relay(0)
+    for r in range(2):
+        slot = lax.rem(y + r, 2)
+        ag_wait(0, slot)
+        norm(0, slot, mix_gain)
+    spread(2, fs)
+
+    def in_block(block, half):
+        for slot in range(2):
+            uv[half, slot] += jnp.dot(
+                normed[block, slot], g_in[half, block], preferred_element_type=F32
+            )
+
+    gathered_loop(0, in_block)
+    relay(1)
+    cross_over(2)
+
+    for copy in small_local:
+        copy.wait()
+    for i, (_, dst) in enumerate(small):
+        landing = (raw_mix, gain_v, bias_all, tg, tv)[i].at[1 - tp]
+        pltpu.make_async_remote_copy(
+            src_ref=landing, dst_ref=landing, send_sem=s_send.at[i], recv_sem=s_recv.at[i],
+            device_id={"tp": 1 - tp}, device_id_type=MESH,
+        ).wait_recv()
+    per_half, block_len = raw_mix.shape[1], raw_mix.shape[2]
+    group_width = cu // per_half
+    at_row = lax.broadcasted_iota(jnp.int32, (block_len, block_len), 0)
+    at_col = lax.broadcasted_iota(jnp.int32, (block_len, block_len), 1)
+    for half in range(nt):
+        turned = bias_all[half].T
+        lane = lax.broadcasted_iota(jnp.int32, turned.shape, 1)
+        for g in range(per_half):
+            mix_low[half, g] = jnp.where(
+                at_row >= at_col, raw_mix[half, g].astype(F32), 0.0
+            ).astype(BF16)
+            bias_col[half, g] = jnp.sum(
+                jnp.where(lane == quarter * per_half + g, turned, 0.0), axis=1, keepdims=True
+            )
+
+    for slot in range(2):
+        def mix_rows(i, _):
+            rows = pl.ds(pl.multiple_of(i * block_len, block_len), block_len)
+            for half in range(nt):
+                for g in range(per_half):
+                    at = g * group_width
+                    activated = jax.nn.gelu(uv[half, slot, rows, cu + at : cu + at + group_width])
+                    centred = activated - jnp.mean(activated, axis=1, keepdims=True)
+                    spread_sq = jnp.mean(centred * centred, axis=1, keepdims=True)
+                    v_norm = (
+                        centred
+                        * lax.rsqrt(spread_sq + EPS_LN)
+                        * gain_v[half, :, at : at + group_width]
+                    ).astype(BF16)
+                    mixed = (
+                        jnp.dot(mix_low[half, g], v_norm, preferred_element_type=F32)
+                        + bias_col[half, g]
+                    )
+                    hidden[slot, rows, half * cu + at : half * cu + at + group_width] = (
+                        jax.nn.gelu(uv[half, slot, rows, at : at + group_width]) * mixed
+                    ).astype(BF16)
+            return 0
+
+        lax.fori_loop(0, seq // block_len, mix_rows, 0)
+
+    scatter_loop(1, 0, hidden, g_out)
+    relay(2)
+    spread(3, fs)
+    cross_over(3)
+    ag_forward(1)
+    for r in range(2):
+        slot = lax.rem(y + r, 2)
+        ag_wait(1, slot)
+        norm(1, slot, ffn_gain)
+    relay(3)
+
+    def up_block(block, half):
+        for slot in range(2):
+            gv[half, slot, 8:, :] += jnp.dot(
+                normed[block, slot], g_up[half, block], preferred_element_type=F32
+            )
+
+    gathered_loop(2, up_block)
+
+    taps_len = tg.shape[1]
+    chunk = 128
+    for slot in range(2):
+        for half in range(nt):
+            for at in range(0, cf, chunk):
+                gate = jnp.zeros((seq, chunk), F32)
+                value = jnp.zeros((seq, chunk), F32)
+                for k in range(taps_len):
+                    first = 8 - (taps_len - 1) + k
+                    rows = slice(first, first + seq)
+                    gate += tg[half, k : k + 1, at : at + chunk].astype(F32) * gv[
+                        half, slot, rows, at : at + chunk
+                    ]
+                    value += tv[half, k : k + 1, at : at + chunk].astype(F32) * gv[
+                        half, slot, rows, cf + at : cf + at + chunk
+                    ]
+                act[slot, :, half * cf + at : half * cf + at + chunk] = (
+                    jax.nn.gelu(gate) * value
+                ).astype(BF16)
+
+    scatter_loop(3, 1, act, g_dn)
+
+    for k in range(4):
+        for copy in across(k, fs):
+            copy.wait_send()
+    for copy in small_away:
+        copy.wait_send()
+
+    def drain_block(block, _):
+        for k in range(4):
+            d_copy(k, block).wait_send()
+        for turn in range(2):
+            for r, kind, used, _now in cases(block):
+                @pl.when(used)
+                def _():
+                    r_copy(turn, r, block, kind).wait_send()
+        return 0
+
+    lax.fori_loop(0, n, drain_block, 0)
+
+    def drain_gather(i, _):
+        for turn in range(2):
+            ag_copy(turn, i, 0).wait_send()
+            ag_copy(turn, i, 1).wait_send()
+            ag_pass(turn, i).wait_send()
+
+            @pl.when(away)
+            def _():
+                ag_copy(turn, i, 2).wait_send()
+        return 0
+
+    lax.fori_loop(0, per, drain_gather, 0)
+
+    def drain_line(at, _):
+        for k in range(4):
+            for step in (2, -2, 1, -1):
+                @pl.when(inside(step))
+                def _():
+                    z_copy(k, z * ny + at, step).wait_send()
+            for sign, source, used in relays():
+                @pl.when(used)
+                def _():
+                    z_copy(k, source * ny + at, sign).wait_send()
+        return 0
+
+    lax.fori_loop(0, ny, drain_line, 0)
+
+
+def on_plane(
+    tokens,
+    mix_gain,
+    w_u,
+    w_v,
+    norm_gain,
+    mix_weight,
+    mix_bias,
+    w_mix_out,
+    ffn_gain,
+    w_gate,
+    w_value,
+    taps_gate,
+    taps_value,
+    w_down,
+):
+    n, nr, nt = lax.axis_size("fs"), lax.axis_size("rep"), lax.axis_size("tp")
+    seq, own_width = tokens.shape
+    per = n // nt
+    width = own_width // per
+    depth = w_u.shape[0]
+    share = nr * 2
+    cu, cf = w_u.shape[1] // share, w_gate.shape[1] // share
+    groups, block_len = mix_weight.shape[0], mix_weight.shape[1]
+    taps_len = taps_gate.shape[0]
+    vmem, sem, hbm = pltpu.VMEM, pltpu.SemaphoreType.DMA, pl.ANY
+    operands = (
+        (tokens, vmem),
+        (mix_gain[None, :], vmem),
+        (w_u, hbm),
+        (w_v, hbm),
+        (norm_gain[None, :], hbm),
+        (mix_weight, hbm),
+        (mix_bias, hbm),
+        (w_mix_out, hbm),
+        (ffn_gain[None, :], vmem),
+        (w_gate, hbm),
+        (w_value, hbm),
+        (taps_gate, hbm),
+        (taps_value, hbm),
+        (w_down, hbm),
+    )
+    return pl.pallas_call(
+        functools.partial(plane_kernel, n, nr, nt),
+        out_shape=jax.ShapeDtypeStruct((seq, own_width), BF16),
+        in_specs=[pl.BlockSpec(memory_space=space) for _, space in operands],
+        out_specs=pl.BlockSpec(memory_space=vmem),
+        scratch_shapes=[
+            vmem((nt, n, depth, 2 * cu), BF16),
+            vmem((n, nt, cu, width), BF16),
+            vmem((nt, n, depth, 2 * cf), BF16),
+            vmem((n, nt, cf, width), BF16),
+            vmem((2, n, seq, width), BF16),
+            vmem((2, n, seq, width), BF16),
+            vmem((per, seq, width), BF16),
+            vmem((n, 2, seq, width), BF16),
+            vmem((nt, 2, seq, 2 * cu), F32),
+            vmem((2, seq, nt * cu), BF16),
+            vmem((nt, 2, seq + 8, 2 * cf), F32),
+            vmem((2, seq, nt * cf), BF16),
+            vmem((2, n, seq, width), BF16),
+            vmem((2, n, seq, width), BF16),
+            vmem((n, seq, width), BF16),
+            vmem((n, seq, width), BF16),
+            vmem((3, per, seq, width), BF16),
+            vmem((3, per, seq, width), BF16),
+            vmem((nt, groups // share, block_len, block_len), BF16),
+            vmem((nt, groups // share, block_len, block_len), BF16),
+            vmem((nt, 1, cu), F32),
+            vmem((nt, groups, block_len), F32),
+            vmem((nt, groups // share, block_len, 1), F32),
+            vmem((nt, taps_len, cf), BF16),
+            vmem((nt, taps_len, cf), BF16),
+            sem((4, 2)),
+            sem((4, 2)),
+            sem((4, 2)),
+            sem((4, n, 5)),
+            sem((4, n)),
+            sem((4, n)),
+            sem((4, n)),
+            sem((5,)),
+            sem((5,)),
+            sem((5,)),
+            sem((2, 3, per)),
+            sem((2, 2, n)),
+            sem((2, per)),
+            sem((2, 2, n)),
+            sem((2, n)),
+            sem((2, 3, per)),
+        ],
+        compiler_params=pltpu.CompilerParams(
+            collective_id=0, has_side_effects=True, vmem_limit_bytes=67043328
+        ),
+    )(*(array for array, _ in operands))
+
+
+def by_shape(*arrays):
+    n, nr, nt = lax.axis_size("fs"), lax.axis_size("rep"), lax.axis_size("tp")
+    groups, units = arrays[5].shape[0], arrays[9].shape[1]
+    share = nr * 2
+    fits = nr == 2 and nt == 2 and n % 2 == 0 and groups % share == 0 and units % (share * 128) == 0
+    return on_plane(*arrays) if fits else on_device(*arrays)
+
+
 def solution(mesh):
     placed = (
         P(("rep", "fs"), "tp"),
@@ -436,5 +1120,5 @@
         P("tp", "fs"),
     )
     return jax.shard_map(
-        on_device, mesh=mesh, in_specs=placed, out_specs=P(("rep", "fs"), "tp"), check_vma=False
+        by_shape, mesh=mesh, in_specs=placed, out_specs=P(("rep", "fs"), "tp"), check_vma=False
     )

time: 228 us -> 184 us (0.81)
  Pallas kernels: 215 us -> 181 us
  local copies, waits for them, and re-layouts: 8.26 us -> 2.06 us
  other arithmetic: 4.69 us -> 0 us
    pallas_call x1, Pallas kernels: 215 us -> 181 us  [on_plane(): pl.pallas_call(functools.partial(plane_kernel, n, nr, nt), out_shape=jax....]
    dynamic_slice x5 -> x0, local copies, waits for them, and re-layouts: 3.97 us -> none  [own_half(): lax.dynamic_slice_in_dim(array, lax.axis_index('rep') * share, share, axis)]
where the time goes in v1:
time: 184 us
  Pallas kernels  181 us (98%)
  local copies, waits for them, and re-layouts  2.06 us (1%)
    pallas_call x1, Pallas kernels, on_plane(): pl.pallas_call(functools.partial(plane_kernel, n, nr, nt), out_shape=jax....  181 us

profile of v1, /device:TPU:1, one launch (start us, length us, event | category | flops | bytes accessed | tf_op | source)
XLA Modules:
  0.0 183.5 jit_solution(4450057352946428663)
XLA Ops:
  0.0 181.5 %shard_map.136 = bf16[384,1024]{1,0:T(8,128)(2,1)} custom-call(bf16[384,1024]{1,0:T(8,128)(2,1)} %tok.1, f32[1,2048]{1,0:T(1,128)} %bitcast.3, bf16[256,1024]{1,0:T(8,128)(2,1)} %w_u.1, bf16[256,1024]{1,0:T(8,128)(2,1)} %w_v.1, f32[1,1024]{1,0:T(1,128)} %bitcast.5, bf16[8,128,128]{2,1,0:T(8,128)(2,1)} %mixw.1, f32[8,128]{1,0:T(8,128)} %bias.1, ...), custom_call_target="tpu_custom_call" | custom-call | tf_op jit(solution)/shard_map/pallas_call | solution.py:1043
  181.5 2.1 %copy.16 = bf16[384,1024]{1,0:T(8,128)(2,1)} copy(bf16[384,1024]{1,0:T(8,128)(2,1)} %shard_map.136) | data formatting | bytes 1572864

commit v2 on v1

--- a/solution.py
+++ b/solution.py
@@ -423,7 +423,7 @@
     tok, mix_gain, w_u, w_v, norm_gain, mixw, bias, w_out, ffn_gain, w_gate, w_value, taps_g, taps_v, w_dn,
     out,
     g_in, g_out, g_up, g_dn, feat, feat2, mid, normed, uv, hidden, gv, act,
-    part1, part2, inc1, inc2, got1, got2, raw_mix, mix_low, gain_v, bias_all, bias_col, tg, tv,
+    row_scale, squares, part1, part2, inc1, inc2, got1, got2, raw_mix, mix_low, gain_v, bias_all, bias_col, tg, tv,
     l_sem, y_send, y_recv, z_send, z_recv, d_send, d_recv, s_local, s_send, s_recv,
     a_send, a_recv, f_send, r_send, i_recv, t_recv,
 ):
@@ -439,8 +439,11 @@
     home = rep == tp
     away = rep != tp
     cu, cf = g_out.shape[2], g_dn.shape[2]
-    mid_rows = (tok, mid)
+    few = max(1, per // 4)
     feats = (feat, feat2)
+
+    def both(*conditions):
+        return functools.reduce(jnp.logical_and, conditions)
 
     barrier = pltpu.get_barrier_semaphore()
     greeted = [{"tp": 1 - tp}]
@@ -502,8 +505,11 @@
     def inside(step):
         return jnp.logical_and(z + step >= 0, z + step < nz)
 
+    def reach(k):
+        return (1, -1) if k == 0 else (2, -2, 1, -1)
+
     def spread(k, block):
-        for step in (2, -2, 1, -1):
+        for step in reach(k):
             @pl.when(inside(step))
             def _():
                 z_copy(k, block, step).start()
@@ -522,29 +528,35 @@
             copy.wait_recv()
         spread(k, fs_y)
 
-    def relays():
+    def relays(k, far):
         return [
             (sign, z - sign * far, jnp.logical_and(inside(sign), inside(-sign * far)))
             for sign in (1, -1)
-            for far in range(2, nz)
         ]
 
-    def relay(k):
-        for at in range(ny):
-            for sign, source, used in relays():
-                @pl.when(used)
-                def _():
-                    arrive(k, source * ny + at)
-                    z_copy(k, source * ny + at, sign).start()
-
-    def relayed(source):
-        up = jnp.logical_and(z - source >= 2, inside(1))
-        down = jnp.logical_and(source - z >= 2, inside(-1))
+    def nearest(k):
+        return 1 if k == 0 else 2
+
+    def relay(k, far, at):
+        for sign, source, used in relays(k, far):
+            @pl.when(used)
+            def _():
+                arrive(k, source * ny + at)
+                z_copy(k, source * ny + at, sign).start()
+
+    def relay_all(k):
+        for far in range(nearest(k), nz - 1):
+            for at in range(ny):
+                relay(k, far, at)
+
+    def relayed(k, source):
+        up = jnp.logical_and(z - source >= nearest(k), inside(1))
+        down = jnp.logical_and(source - z >= nearest(k), inside(-1))
         return jnp.logical_or(up, down)
 
     def need(k, block):
         source = block // ny
-        @pl.when(jnp.logical_and(source != z, jnp.logical_not(relayed(source))))
+        @pl.when(jnp.logical_and(source != z, jnp.logical_not(relayed(k, source))))
         def _():
             arrive(k, block)
 
@@ -611,12 +623,17 @@
         def _():
             feats[turn][y, tp * per + i] = ag_source(turn, i)[...]
 
-    def ag_pass(turn, i):
+    def passed(block):
+        at = lax.rem(block, per)
+        return jnp.logical_or(
+            jnp.logical_and(home, at >= few), jnp.logical_and(away, at < few)
+        )
+
+    def ag_pass(turn, block):
         slot = jnp.where(home, 1 - y, y)
-        block = jnp.where(home, (nt - 1) * per, 0) + i
         return pltpu.make_async_remote_copy(
             src_ref=feats[turn].at[slot, block], dst_ref=feats[turn].at[slot, block],
-            send_sem=f_send.at[turn, i], recv_sem=a_recv.at[turn, slot, block],
+            send_sem=f_send.at[turn, block], recv_sem=a_recv.at[turn, slot, block],
             device_id={
                 "rep": jnp.where(home, 1 - rep, rep),
                 "fs": jnp.where(home, fs, fs_y),
@@ -631,52 +648,40 @@
             recv_sem=a_recv.at[turn, slot, block], device_id={"tp": 1 - tp}, device_id_type=MESH,
         ).wait_recv()
 
-    def ag_forward(turn):
-        def step(i, _):
-            slot = jnp.where(home, 1 - y, y)
-            ag_landed(turn, slot, jnp.where(home, (nt - 1) * per, 0) + i)
-            ag_pass(turn, i).start()
-            return 0
-
-        lax.fori_loop(0, per, step, 0)
-
-    def ag_wait(turn, slot):
-        def step(block, _):
-            half = block // per
-            local = jnp.logical_and(home, jnp.logical_and(slot == y, half == tp))
-            passed_home = jnp.logical_and(home, jnp.logical_and(slot != y, half == nt - 1))
-            passed_away = jnp.logical_and(away, jnp.logical_and(slot == y, half == 0))
-            done = jnp.logical_or(local, jnp.logical_or(passed_home, passed_away))
-
-            @pl.when(jnp.logical_not(done))
-            def _():
-                ag_landed(turn, slot, block)
-
-            return 0
-
-        lax.fori_loop(0, n, step, 0)
-
-    def norm(turn, slot, gain):
-        slabs = feats[turn]
-
-        def add(block, total):
-            values = slabs[slot, block].astype(F32)
-            return total + jnp.sum(values * values, axis=1, keepdims=True)
-
-        total = lax.fori_loop(0, n, add, jnp.zeros((seq, 1), F32))
-        scale = lax.rsqrt(total / (n * width) + EPS_RMS)
-
-        def put(block, _):
-            values = slabs[slot, block].astype(F32)
-            cols = pl.ds(pl.multiple_of(block * width, 128), width)
-            normed[block, slot] = (values * scale * gain[:, cols]).astype(BF16)
-            return 0
-
-        lax.fori_loop(0, n, put, 0)
-
-    def gathered_loop(k, multiply):
+    def ag_forward(turn, block):
+        @pl.when(passed(block))
+        def _():
+            ag_landed(turn, jnp.where(home, 1 - y, y), block)
+            ag_pass(turn, block).start()
+
+    def ag_wait(turn, slot, block):
+        local = both(home, slot == y, block // per == tp)
+        sent_on = jnp.logical_and(passed(block), slot == jnp.where(home, 1 - y, y))
+
+        @pl.when(jnp.logical_not(jnp.logical_or(local, sent_on)))
+        def _():
+            ag_landed(turn, slot, block)
+
+    def weigh(turn, gain, block):
+        gains = gain[:, pl.ds(pl.multiple_of(block * width, 128), width)]
+        for r in range(2):
+            slot = lax.rem(y + r, 2)
+            ag_wait(turn, slot, block)
+            values = feats[turn][slot, block].astype(F32)
+            normed[block, slot] = (values * gains).astype(BF16)
+            for at in range(0, width, 128):
+                piece = values[:, at : at + 128]
+                squares[slot] += piece * piece
+
+    def finish_scale():
+        for slot in range(2):
+            total = jnp.sum(squares[slot], axis=1, keepdims=True)
+            row_scale[slot, 8:, :] = lax.rsqrt(total / (n * width) + EPS_RMS)
+
+    def gathered_loop(k, turn, gain, multiply):
         def step(i, _):
             block = near_block(i)
+            weigh(turn, gain, block)
             need(k, block)
             multiply(block, tp)
 
@@ -692,12 +697,10 @@
         last = near_block(n - 1)
         partner_wait(k, last)
         multiply(last, 1 - tp)
+        finish_scale()
 
     def even(block):
         return lax.rem(block, 2) == 0
-
-    def both(*conditions):
-        return functools.reduce(jnp.logical_and, conditions)
 
     parts, incs, gots = (part1, part2), (inc1, inc2), (got1, got2)
 
@@ -788,7 +791,7 @@
         else:
             out[:, cols] = (mid[at].astype(F32) + total).astype(BF16)
 
-    def scatter_loop(k, turn, left, weight):
+    def scatter_loop(k, turn, left, weight, beside):
         def step(i, _):
             @pl.when(i < n)
             def _():
@@ -803,6 +806,9 @@
             @pl.when(both(i >= 3, i < n + 3))
             def _():
                 join(turn, plain_block(i - 3))
+
+            for at, action in beside:
+                pl.when(i == at)(action)
 
             @pl.when(i >= 5)
             def _():
@@ -829,29 +835,32 @@
         copy.start()
     for i in range(per):
         ag_send(0, i)
-    for k in range(2):
+    for copy in own_load(0):
+        copy.wait()
+    spread(0, fs)
+    for copy in across(1, fs) + small_away:
+        copy.start()
+    uv[...] = jnp.zeros_like(uv)
+    gv[...] = jnp.zeros_like(gv)
+    squares[...] = jnp.zeros_like(squares)
+    row_scale[...] = jnp.zeros_like(row_scale)
+    cross_over(0)
+    for k in range(1, 4):
         for copy in own_load(k):
             copy.wait()
-        spread(k, fs)
-    for copy in across(1, fs) + small_away:
-        copy.start()
-    cross_over(0)
-    for k in (2, 3):
-        for copy in own_load(k):
-            copy.wait()
-    ag_forward(0)
+    turns = [(far, at) for far in range(1, nz - 1) for at in (y, 1 - y)]
+    for i in range(max(per, len(turns))):
+        if i < len(turns):
+            relay(0, *turns[i])
+        if i == 2:
+            spread(1, fs)
+        if i < per:
+            for half in range(nt):
+                ag_forward(0, half * per + i)
     cross_over(1)
     for k in (2, 3):
         for copy in across(k, fs):
             copy.start()
-    uv[...] = jnp.zeros_like(uv)
-    gv[...] = jnp.zeros_like(gv)
-    relay(0)
-    for r in range(2):
-        slot = lax.rem(y + r, 2)
-        ag_wait(0, slot)
-        norm(0, slot, mix_gain)
-    spread(2, fs)
 
     def in_block(block, half):
         for slot in range(2):
@@ -859,9 +868,7 @@
                 normed[block, slot], g_in[half, block], preferred_element_type=F32
             )
 
-    gathered_loop(0, in_block)
-    relay(1)
-    cross_over(2)
+    gathered_loop(0, 0, mix_gain, in_block)
 
     for copy in small_local:
         copy.wait()
@@ -889,10 +896,13 @@
     for slot in range(2):
         def mix_rows(i, _):
             rows = pl.ds(pl.multiple_of(i * block_len, block_len), block_len)
+            scale = row_scale[slot, pl.ds(pl.multiple_of(i * block_len + 8, 8), block_len), :]
             for half in range(nt):
                 for g in range(per_half):
                     at = g * group_width
-                    activated = jax.nn.gelu(uv[half, slot, rows, cu + at : cu + at + group_width])
+                    activated = jax.nn.gelu(
+                        uv[half, slot, rows, cu + at : cu + at + group_width] * scale
+                    )
                     centred = activated - jnp.mean(activated, axis=1, keepdims=True)
                     spread_sq = jnp.mean(centred * centred, axis=1, keepdims=True)
                     v_norm = (
@@ -905,22 +915,23 @@
                         + bias_col[half, g]
                     )
                     hidden[slot, rows, half * cu + at : half * cu + at + group_width] = (
-                        jax.nn.gelu(uv[half, slot, rows, at : at + group_width]) * mixed
+                        jax.nn.gelu(uv[half, slot, rows, at : at + group_width] * scale) * mixed
                     ).astype(BF16)
             return 0
 
         lax.fori_loop(0, seq // block_len, mix_rows, 0)
 
-    scatter_loop(1, 0, hidden, g_out)
-    relay(2)
-    spread(3, fs)
-    cross_over(3)
-    ag_forward(1)
-    for r in range(2):
-        slot = lax.rem(y + r, 2)
-        ag_wait(1, slot)
-        norm(1, slot, ffn_gain)
-    relay(3)
+    relay_all(1)
+    spread(2, fs)
+    cross_over(2)
+    squares[...] = jnp.zeros_like(squares)
+
+    def start_down():
+        spread(3, fs)
+        cross_over(3)
+
+    scatter_loop(1, 0, hidden, g_out, ((n + 2, lambda: relay_all(2)), (n + 3, start_down)))
+    lax.fori_loop(0, n, lambda i, _: (ag_forward(1, plain_block(i)), 0)[1], 0)
 
     def up_block(block, half):
         for slot in range(2):
@@ -928,7 +939,8 @@
                 normed[block, slot], g_up[half, block], preferred_element_type=F32
             )
 
-    gathered_loop(2, up_block)
+    gathered_loop(2, 1, ffn_gain, up_block)
+    relay_all(3)
 
     taps_len = tg.shape[1]
     chunk = 128
@@ -940,17 +952,18 @@
                 for k in range(taps_len):
                     first = 8 - (taps_len - 1) + k
                     rows = slice(first, first + seq)
-                    gate += tg[half, k : k + 1, at : at + chunk].astype(F32) * gv[
-                        half, slot, rows, at : at + chunk
-                    ]
-                    value += tv[half, k : k + 1, at : at + chunk].astype(F32) * gv[
-                        half, slot, rows, cf + at : cf + at + chunk
-                    ]
+                    scale = row_scale[slot, rows, :]
+                    gate += tg[half, k : k + 1, at : at + chunk].astype(F32) * (
+                        gv[half, slot, rows, at : at + chunk] * scale
+                    )
+                    value += tv[half, k : k + 1, at : at + chunk].astype(F32) * (
+                        gv[half, slot, rows, cf + at : cf + at + chunk] * scale
+                    )
                 act[slot, :, half * cf + at : half * cf + at + chunk] = (
                     jax.nn.gelu(gate) * value
                 ).astype(BF16)
 
-    scatter_loop(3, 1, act, g_dn)
+    scatter_loop(3, 1, act, g_dn, ())
 
     for k in range(4):
         for copy in across(k, fs):
@@ -966,6 +979,10 @@
                 @pl.when(used)
                 def _():
                     r_copy(turn, r, block, kind).wait_send()
+
+            @pl.when(passed(block))
+            def _():
+                ag_pass(turn, block).wait_send()
         return 0
 
     lax.fori_loop(0, n, drain_block, 0)
@@ -974,7 +991,6 @@
         for turn in range(2):
             ag_copy(turn, i, 0).wait_send()
             ag_copy(turn, i, 1).wait_send()
-            ag_pass(turn, i).wait_send()
 
             @pl.when(away)
             def _():
@@ -985,14 +1001,15 @@
 
     def drain_line(at, _):
         for k in range(4):
-            for step in (2, -2, 1, -1):
+            for step in reach(k):
                 @pl.when(inside(step))
                 def _():
                     z_copy(k, z * ny + at, step).wait_send()
-            for sign, source, used in relays():
-                @pl.when(used)
-                def _():
-                    z_copy(k, source * ny + at, sign).wait_send()
+            for far in range(nearest(k), nz - 1):
+                for sign, source, used in relays(k, far):
+                    @pl.when(used)
+                    def _():
+                        z_copy(k, source * ny + at, sign).wait_send()
         return 0
 
     lax.fori_loop(0, ny, drain_line, 0)
@@ -1058,6 +1075,8 @@
             vmem((2, seq, nt * cu), BF16),
             vmem((nt, 2, seq + 8, 2 * cf), F32),
             vmem((2, seq, nt * cf), BF16),
+            vmem((2, seq + 8, 1), F32),
+            vmem((2, seq, 128), F32),
             vmem((2, n, seq, width), BF16),
             vmem((2, n, seq, width), BF16),
             vmem((n, seq, width), BF16),
@@ -1083,7 +1102,7 @@
             sem((5,)),
             sem((2, 3, per)),
             sem((2, 2, n)),
-            sem((2, per)),
+            sem((2, n)),
             sem((2, 2, n)),
             sem((2, n)),
             sem((2, 3, per)),

time: 184 us -> 174 us (0.946)
  Pallas kernels: 181 us -> 170 us
    pallas_call x1, Pallas kernels: 181 us -> 170 us  [on_plane(): pl.pallas_call(functools.partial(plane_kernel, n, nr, nt), out_shape=jax....]
where the time goes in v2:
time: 174 us; the launch traced here: 172 us
  Pallas kernels  170 us (98%)
  local copies, waits for them, and re-layouts  2.06 us (1%)
    pallas_call x1, Pallas kernels, on_plane(): pl.pallas_call(functools.partial(plane_kernel, n, nr, nt), out_shape=jax....  170 us

profile of v2, /device:TPU:1, one launch (start us, length us, event | category | flops | bytes accessed | tf_op | source)
XLA Modules:
  0.0 171.8 jit_solution(3373350650223080162)
XLA Ops:
  0.0 169.7 %shard_map.136 = bf16[384,1024]{1,0:T(8,128)(2,1)} custom-call(bf16[384,1024]{1,0:T(8,128)(2,1)} %tok.1, f32[1,2048]{1,0:T(1,128)} %bitcast.3, bf16[256,1024]{1,0:T(8,128)(2,1)} %w_u.1, bf16[256,1024]{1,0:T(8,128)(2,1)} %w_v.1, f32[1,1024]{1,0:T(1,128)} %bitcast.5, bf16[8,128,128]{2,1,0:T(8,128)(2,1)} %mixw.1, f32[8,128]{1,0:T(8,128)} %bias.1, ...), custom_call_target="tpu_custom_call" | custom-call | tf_op jit(solution)/shard_map/pallas_call | solution.py:1060
  169.8 2.1 %copy.16 = bf16[384,1024]{1,0:T(8,128)(2,1)} copy(bf16[384,1024]{1,0:T(8,128)(2,1)} %shard_map.136) | data formatting | bytes 1572864

commit v3 on v2

--- a/solution.py
+++ b/solution.py
@@ -439,7 +439,8 @@
     home = rep == tp
     away = rep != tp
     cu, cf = g_out.shape[2], g_dn.shape[2]
-    few = max(1, per // 4)
+    depth = w_u.shape[0]
+    few = (max(1, per // 4), max(1, per // 2))
     feats = (feat, feat2)
 
     def both(*conditions):
@@ -452,12 +453,11 @@
     greeted += [{"fs": lax.rem(z + k, nz) * ny + y} for k in range(1, nz)]
 
     def item(k, block, half):
-        if k == 0:
-            return g_in.at[half, block]
+        if k in (0, 2):
+            rows = pl.ds(pl.multiple_of(block * depth, 128), depth)
+            return (g_in if k == 0 else g_up).at[half, rows]
         if k == 1:
             return g_out.at[block, half]
-        if k == 2:
-            return g_up.at[half, block]
         return g_dn.at[block, half]
 
     def pieces(k, which, block):
@@ -491,7 +491,7 @@
     def z_copy(k, block, step):
         return pltpu.make_async_remote_copy(
             src_ref=item(k, block, tp), dst_ref=item(k, block, tp),
-            send_sem=z_send.at[k, block, step + 2], recv_sem=z_recv.at[k, block],
+            send_sem=z_send.at[k, block, (step + 1) // 2], recv_sem=z_recv.at[k, block],
             device_id={"fs": fs + ny * step}, device_id_type=MESH,
         )
 
@@ -505,11 +505,8 @@
     def inside(step):
         return jnp.logical_and(z + step >= 0, z + step < nz)
 
-    def reach(k):
-        return (1, -1) if k == 0 else (2, -2, 1, -1)
-
     def spread(k, block):
-        for step in reach(k):
+        for step in (1, -1):
             @pl.when(inside(step))
             def _():
                 z_copy(k, block, step).start()
@@ -518,7 +515,7 @@
     def arrive(k, block):
         landing = item(k, block, tp)
         pltpu.make_async_remote_copy(
-            src_ref=landing, dst_ref=landing, send_sem=z_send.at[k, block, 2],
+            src_ref=landing, dst_ref=landing, send_sem=z_send.at[k, block, 0],
             recv_sem=z_recv.at[k, block], device_id={"tp": 1 - tp}, device_id_type=MESH,
         ).wait_recv()
         d_copy(k, block).start()
@@ -528,35 +525,32 @@
             copy.wait_recv()
         spread(k, fs_y)
 
-    def relays(k, far):
+    def relays(far):
         return [
             (sign, z - sign * far, jnp.logical_and(inside(sign), inside(-sign * far)))
             for sign in (1, -1)
         ]
 
-    def nearest(k):
-        return 1 if k == 0 else 2
-
     def relay(k, far, at):
-        for sign, source, used in relays(k, far):
+        for sign, source, used in relays(far):
             @pl.when(used)
             def _():
                 arrive(k, source * ny + at)
                 z_copy(k, source * ny + at, sign).start()
 
-    def relay_all(k):
-        for far in range(nearest(k), nz - 1):
-            for at in range(ny):
+    def relay_from(k, first, last):
+        for far in range(first, last):
+            for at in (y, 1 - y):
                 relay(k, far, at)
 
-    def relayed(k, source):
-        up = jnp.logical_and(z - source >= nearest(k), inside(1))
-        down = jnp.logical_and(source - z >= nearest(k), inside(-1))
+    def relayed(source):
+        up = jnp.logical_and(z > source, inside(1))
+        down = jnp.logical_and(source > z, inside(-1))
         return jnp.logical_or(up, down)
 
     def need(k, block):
         source = block // ny
-        @pl.when(jnp.logical_and(source != z, jnp.logical_not(relayed(k, source))))
+        @pl.when(jnp.logical_and(source != z, jnp.logical_not(relayed(source))))
         def _():
             arrive(k, block)
 
@@ -572,9 +566,6 @@
         swing = z + ((i + 1) // 2) * (1 - 2 * (i % 2))
         rest = jnp.where(z < nz - 1 - z, i, nz - 1 - i)
         return jnp.where(i <= 2 * near, swing, rest)
-
-    def near_block(i):
-        return order(i // ny) * ny + lax.rem(y + i, ny)
 
     def plain_block(i):
         return order(i // ny) * ny + lax.rem(i, ny)
@@ -623,10 +614,10 @@
         def _():
             feats[turn][y, tp * per + i] = ag_source(turn, i)[...]
 
-    def passed(block):
+    def passed(turn, block):
         at = lax.rem(block, per)
         return jnp.logical_or(
-            jnp.logical_and(home, at >= few), jnp.logical_and(away, at < few)
+            jnp.logical_and(home, at >= few[turn]), jnp.logical_and(away, at < few[turn])
         )
 
     def ag_pass(turn, block):
@@ -649,14 +640,14 @@
         ).wait_recv()
 
     def ag_forward(turn, block):
-        @pl.when(passed(block))
+        @pl.when(passed(turn, block))
         def _():
             ag_landed(turn, jnp.where(home, 1 - y, y), block)
             ag_pass(turn, block).start()
 
     def ag_wait(turn, slot, block):
         local = both(home, slot == y, block // per == tp)
-        sent_on = jnp.logical_and(passed(block), slot == jnp.where(home, 1 - y, y))
+        sent_on = jnp.logical_and(passed(turn, block), slot == jnp.where(home, 1 - y, y))
 
         @pl.when(jnp.logical_not(jnp.logical_or(local, sent_on)))
         def _():
@@ -668,7 +659,10 @@
             slot = lax.rem(y + r, 2)
             ag_wait(turn, slot, block)
             values = feats[turn][slot, block].astype(F32)
-            normed[block, slot] = (values * gains).astype(BF16)
+            rows = pl.ds(pl.multiple_of(slot * seq, 8), seq)
+            normed[rows, pl.ds(pl.multiple_of(block * width, 128), width)] = (
+                values * gains
+            ).astype(BF16)
             for at in range(0, width, 128):
                 piece = values[:, at : at + 128]
                 squares[slot] += piece * piece
@@ -678,25 +672,40 @@
             total = jnp.sum(squares[slot], axis=1, keepdims=True)
             row_scale[slot, 8:, :] = lax.rsqrt(total / (n * width) + EPS_RMS)
 
-    def gathered_loop(k, turn, gain, multiply):
+    def gathered_loop(k, turn, gain, multiply, lead, beside):
+        def arrived(source, half):
+            if half is tp:
+                for at in range(ny):
+                    weigh(turn, gain, source * ny + at)
+                for at in (y, 1 - y):
+                    need(k, source * ny + at)
+            else:
+                for at in (y, 1 - y):
+                    partner_wait(k, source * ny + at)
+            cols = pl.ds(pl.multiple_of(source * ny * depth, 128), ny * depth)
+            multiply(cols, half)
+
         def step(i, _):
-            block = near_block(i)
-            weigh(turn, gain, block)
-            need(k, block)
-            multiply(block, tp)
-
-            @pl.when(i > 0)
-            def _():
-                before = near_block(i - 1)
-                partner_wait(k, before)
-                multiply(before, 1 - tp)
+            if lead:
+                @pl.when(i < nz)
+                def _():
+                    for at in range(ny):
+                        ag_forward(turn, order(i) * ny + at)
+
+            for at, action in beside:
+                pl.when(i == at)(action)
+
+            @pl.when(both(i >= lead, i < nz + lead))
+            def _():
+                arrived(order(i - lead), tp)
+
+            @pl.when(i >= lead + 1)
+            def _():
+                arrived(order(i - lead - 1), 1 - tp)
 
             return 0
 
-        lax.fori_loop(0, n, step, 0)
-        last = near_block(n - 1)
-        partner_wait(k, last)
-        multiply(last, 1 - tp)
+        lax.fori_loop(0, nz + lead + 1, step, 0)
         finish_scale()
 
     def even(block):
@@ -852,23 +861,20 @@
     for i in range(max(per, len(turns))):
         if i < len(turns):
             relay(0, *turns[i])
-        if i == 2:
-            spread(1, fs)
         if i < per:
             for half in range(nt):
                 ag_forward(0, half * per + i)
+    spread(1, fs)
     cross_over(1)
     for k in (2, 3):
         for copy in across(k, fs):
             copy.start()
 
-    def in_block(block, half):
-        for slot in range(2):
-            uv[half, slot] += jnp.dot(
-                normed[block, slot], g_in[half, block], preferred_element_type=F32
-            )
-
-    gathered_loop(0, 0, mix_gain, in_block)
+    def in_block(cols, half):
+        uv[half] += jnp.dot(normed[:, cols], g_in[half, cols], preferred_element_type=F32)
+
+    gathered_loop(0, 0, mix_gain, in_block, 0, ())
+    relay_from(1, 1, 2)
 
     for copy in small_local:
         copy.wait()
@@ -895,13 +901,14 @@
 
     for slot in range(2):
         def mix_rows(i, _):
-            rows = pl.ds(pl.multiple_of(i * block_len, block_len), block_len)
+            own_rows = pl.ds(pl.multiple_of(i * block_len, block_len), block_len)
+            rows = pl.ds(pl.multiple_of(slot * seq + i * block_len, block_len), block_len)
             scale = row_scale[slot, pl.ds(pl.multiple_of(i * block_len + 8, 8), block_len), :]
             for half in range(nt):
                 for g in range(per_half):
                     at = g * group_width
                     activated = jax.nn.gelu(
-                        uv[half, slot, rows, cu + at : cu + at + group_width] * scale
+                        uv[half, rows, cu + at : cu + at + group_width] * scale
                     )
                     centred = activated - jnp.mean(activated, axis=1, keepdims=True)
                     spread_sq = jnp.mean(centred * centred, axis=1, keepdims=True)
@@ -914,14 +921,14 @@
                         jnp.dot(mix_low[half, g], v_norm, preferred_element_type=F32)
                         + bias_col[half, g]
                     )
-                    hidden[slot, rows, half * cu + at : half * cu + at + group_width] = (
-                        jax.nn.gelu(uv[half, slot, rows, at : at + group_width] * scale) * mixed
+                    hidden[slot, own_rows, half * cu + at : half * cu + at + group_width] = (
+                        jax.nn.gelu(uv[half, rows, at : at + group_width] * scale) * mixed
                     ).astype(BF16)
             return 0
 
         lax.fori_loop(0, seq // block_len, mix_rows, 0)
 
-    relay_all(1)
+    relay_from(1, 2, nz - 1)
     spread(2, fs)
     cross_over(2)
     squares[...] = jnp.zeros_like(squares)
@@ -930,17 +937,20 @@
         spread(3, fs)
         cross_over(3)
 
-    scatter_loop(1, 0, hidden, g_out, ((n + 2, lambda: relay_all(2)), (n + 3, start_down)))
-    lax.fori_loop(0, n, lambda i, _: (ag_forward(1, plain_block(i)), 0)[1], 0)
-
-    def up_block(block, half):
+    hops = (
+        (n // 2 + 1, lambda: relay(2, 1, y)),
+        (n // 2 + 2, lambda: relay(2, 1, 1 - y)),
+        (n, lambda: relay_from(2, 2, nz - 1)),
+        (n + 3, start_down),
+    )
+    scatter_loop(1, 0, hidden, g_out, hops)
+
+    def up_block(cols, half):
+        product = jnp.dot(normed[:, cols], g_up[half, cols], preferred_element_type=F32)
         for slot in range(2):
-            gv[half, slot, 8:, :] += jnp.dot(
-                normed[block, slot], g_up[half, block], preferred_element_type=F32
-            )
-
-    gathered_loop(2, 1, ffn_gain, up_block)
-    relay_all(3)
+            gv[half, slot, 8:, :] += product[slot * seq : (slot + 1) * seq]
+
+    gathered_loop(2, 1, ffn_gain, up_block, 1, ((nz - 1, lambda: relay_from(3, 1, 2)),))
 
     taps_len = tg.shape[1]
     chunk = 128
@@ -963,6 +973,7 @@
                     jax.nn.gelu(gate) * value
                 ).astype(BF16)
 
+    relay_from(3, 2, nz - 1)
     scatter_loop(3, 1, act, g_dn, ())
 
     for k in range(4):
@@ -980,7 +991,7 @@
                 def _():
                     r_copy(turn, r, block, kind).wait_send()
 
-            @pl.when(passed(block))
+            @pl.when(passed(turn, block))
             def _():
                 ag_pass(turn, block).wait_send()
         return 0
@@ -1001,12 +1012,12 @@
 
     def drain_line(at, _):
         for k in range(4):
-            for step in reach(k):
+            for step in (1, -1):
                 @pl.when(inside(step))
                 def _():
                     z_copy(k, z * ny + at, step).wait_send()
-            for far in range(nearest(k), nz - 1):
-                for sign, source, used in relays(k, far):
+            for far in range(1, nz - 1):
+                for sign, source, used in relays(far):
                     @pl.when(used)
                     def _():
                         z_copy(k, source * ny + at, sign).wait_send()
@@ -1063,15 +1074,15 @@
         in_specs=[pl.BlockSpec(memory_space=space) for _, space in operands],
         out_specs=pl.BlockSpec(memory_space=vmem),
         scratch_shapes=[
-            vmem((nt, n, depth, 2 * cu), BF16),
+            vmem((nt, n * depth, 2 * cu), BF16),
             vmem((n, nt, cu, width), BF16),
-            vmem((nt, n, depth, 2 * cf), BF16),
+            vmem((nt, n * depth, 2 * cf), BF16),
             vmem((n, nt, cf, width), BF16),
             vmem((2, n, seq, width), BF16),
             vmem((2, n, seq, width), BF16),
             vmem((per, seq, width), BF16),
-            vmem((n, 2, seq, width), BF16),
-            vmem((nt, 2, seq, 2 * cu), F32),
+            vmem((2 * seq, n * width), BF16),
+            vmem((nt, 2 * seq, 2 * cu), F32),
             vmem((2, seq, nt * cu), BF16),
             vmem((nt, 2, seq + 8, 2 * cf), F32),
             vmem((2, seq, nt * cf), BF16),
@@ -1093,7 +1104,7 @@
             sem((4, 2)),
             sem((4, 2)),
             sem((4, 2)),
-            sem((4, n, 5)),
+            sem((4, n, 2)),
             sem((4, n)),
             sem((4, n)),
             sem((4, n)),

time: 174 us -> 157 us (0.902); the launches traced: 172 us -> 157 us
  Pallas kernels: 170 us -> 155 us
    pallas_call x1, Pallas kernels: 170 us -> 155 us  [on_plane(): pl.pallas_call(functools.partial(plane_kernel, n, nr, nt), out_shape=jax....]
where the time goes in v3:
time: 157 us
  Pallas kernels  155 us (99%)
  local copies, waits for them, and re-layouts  2.06 us (1%)
    pallas_call x1, Pallas kernels, on_plane(): pl.pallas_call(functools.partial(plane_kernel, n, nr, nt), out_shape=jax....  155 us

profile of v3, /device:TPU:1, one launch (start us, length us, event | category | flops | bytes accessed | tf_op | source)
XLA Modules:
  0.0 157.2 jit_solution(12854791564701679799)
XLA Ops:
  0.0 155.2 %shard_map.136 = bf16[384,1024]{1,0:T(8,128)(2,1)} custom-call(bf16[384,1024]{1,0:T(8,128)(2,1)} %tok.1, f32[1,2048]{1,0:T(1,128)} %bitcast.3, bf16[256,1024]{1,0:T(8,128)(2,1)} %w_u.1, bf16[256,1024]{1,0:T(8,128)(2,1)} %w_v.1, f32[1,1024]{1,0:T(1,128)} %bitcast.5, bf16[8,128,128]{2,1,0:T(8,128)(2,1)} %mixw.1, f32[8,128]{1,0:T(8,128)} %bias.1, ...), custom_call_target="tpu_custom_call" | custom-call | tf_op jit(solution)/shard_map/pallas_call | solution.py:1071
  155.2 2.1 %copy.16 = bf16[384,1024]{1,0:T(8,128)(2,1)} copy(bf16[384,1024]{1,0:T(8,128)(2,1)} %shard_map.136) | data formatting | bytes 1572864

commit v4 on v3

--- a/solution.py
+++ b/solution.py
@@ -12,6 +12,7 @@
 F32 = jnp.float32
 BF16 = jnp.bfloat16
 MESH = pl.DeviceIdType.MESH
+STRAIGHT = (0, 1)
 
 
 def own_half(array, axis):
@@ -420,15 +421,15 @@
 
 def plane_kernel(
     n, nr, nt,
-    tok, mix_gain, w_u, w_v, norm_gain, mixw, bias, w_out, ffn_gain, w_gate, w_value, taps_g, taps_v, w_dn,
-    out,
-    g_in, g_out, g_up, g_dn, feat, feat2, mid, normed, uv, hidden, gv, act,
-    row_scale, squares, part1, part2, inc1, inc2, got1, got2, raw_mix, mix_low, gain_v, bias_all, bias_col, tg, tv,
-    l_sem, y_send, y_recv, z_send, z_recv, d_send, d_recv, s_local, s_send, s_recv,
+    tok_hbm, mix_gain_hbm, w_u, w_v, norm_gain, mixw, bias, w_out, ffn_gain_hbm, w_gate, w_value, taps_g, taps_v, w_dn,
+    out_hbm,
+    tok, out, mix_gain, ffn_gain, g_in, g_out, g_up, g_dn, feat, feat2, mid, normed, uv, hidden, gv, act,
+    row_scale, squares, extra, part1, part2, inc1, inc2, got1, got2, raw_mix, mix_low, gain_v, bias_all, bias_col, tg, tv,
+    t_sem, o_sem, n_sem, l_sem, y_send, y_recv, z_send, z_recv, d_send, d_recv, s_local, s_send, s_recv,
     a_send, a_recv, f_send, r_send, i_recv, t_recv,
 ):
     rep, fs, tp = lax.axis_index("rep"), lax.axis_index("fs"), lax.axis_index("tp")
-    seq, own_width = tok.shape
+    seq, own_width = tok_hbm.shape
     ny, nz = 2, n // 2
     z, y = fs // ny, fs % ny
     per = n // nt
@@ -450,6 +451,7 @@
     greeted = [{"tp": 1 - tp}]
     greeted += [{"rep": 1 - rep, "tp": t} for t in range(nt)]
     greeted += [{"fs": fs_y, "tp": t} for t in range(nt)]
+    greeted += [{"rep": 1 - rep, "fs": fs_y, "tp": t} for t in range(nt)]
     greeted += [{"fs": lax.rem(z + k, nz) * ny + y} for k in range(1, nz)]
 
     def item(k, block, half):
@@ -540,7 +542,7 @@
 
     def relay_from(k, first, last):
         for far in range(first, last):
-            for at in (y, 1 - y):
+            for at in range(ny):
                 relay(k, far, at)
 
     def relayed(source):
@@ -588,10 +590,17 @@
         for i, (src, dst) in enumerate(small)
     ]
 
+    def columns(i):
+        return pl.ds(pl.multiple_of(i * width, 128), width)
+
+    def tok_load(i):
+        return pltpu.make_async_copy(tok_hbm.at[:, columns(i)], tok.at[i], t_sem.at[i])
+
+    def out_store(i):
+        return pltpu.make_async_copy(out.at[i], out_hbm.at[:, columns(i)], o_sem.at[i])
+
     def ag_source(turn, i):
-        if turn == 0:
-            return tok.at[:, pl.ds(pl.multiple_of(i * width, 128), width)]
-        return mid.at[i]
+        return (tok, mid)[turn].at[i]
 
     def ag_copy(turn, i, way):
         block = tp * per + i
@@ -723,43 +732,65 @@
             "pair": (got.at[0, at], t_recv.at[turn, 0, at], {"tp": 1 - tp}),
             "x": (got.at[1, at], t_recv.at[turn, 1, at], {"rep": 1 - rep, "tp": core}),
             "y": (got.at[2, at], t_recv.at[turn, 2, at], {"fs": fs_y, "tp": core}),
+            "diag": (
+                got.at[3, at], t_recv.at[turn, 3, at],
+                {"rep": 1 - rep, "fs": fs_y, "tp": core},
+            ),
         }[kind]
         return pltpu.make_async_remote_copy(
             src_ref=parts[turn].at[slot, block], dst_ref=dst, send_sem=r_send.at[turn, r, block],
             recv_sem=sem, device_id=device, device_id_type=MESH,
         )
 
-    def cases(block):
+    def straight(turn, block):
+        hit = block == plain_block(n - 1)
+        for i in range(n - STRAIGHT[turn], n - 1):
+            hit = jnp.logical_or(hit, block == plain_block(i))
+        return hit if STRAIGHT[turn] else block < 0
+
+    def cases(turn, block):
+        once = straight(turn, block)
+        twice = jnp.logical_not(once)
+        is_even = even(block)
+        is_odd = jnp.logical_not(is_even)
         return (
-            (1, "diag_x", both(away, even(block)), True),
-            (1, "diag_y", both(away, jnp.logical_not(even(block))), True),
-            (1, "y", both(home, jnp.logical_not(even(block))), True),
+            (1, "diag_x", both(away, twice, is_even), True),
+            (1, "diag_y", both(away, twice, is_odd), True),
+            (1, "diag", both(away, once), True),
+            (1, "y", both(home, jnp.logical_or(once, is_odd)), True),
             (0, "pair", both(home, block // per != tp), True),
-            (0, "x", both(away, even(block)), True),
-            (1, "y", both(home, even(block)), False),
-            (0, "x", both(away, jnp.logical_not(even(block))), False),
+            (0, "x", both(away, jnp.logical_or(once, is_even)), True),
+            (1, "y", both(home, twice, is_even), False),
+            (0, "x", both(away, twice, is_odd), False),
         )
 
-    def project(turn, left, weight, block):
+    def project(turn, left, weight, block, r):
         size = weight.shape[1] * weight.shape[2]
         right = weight[block].reshape(size, weight.shape[3])
-        for r in (1, 0):
-            slot = lax.rem(y + r, 2)
-            parts[turn][slot, block] = jnp.dot(
-                left[slot], right, preferred_element_type=F32
-            ).astype(BF16)
-            for row, kind, used, now in cases(block):
-                if row == r and now:
-                    @pl.when(used)
-                    def _():
-                        r_copy(turn, r, block, kind).start()
-
-        @pl.when(both(home, block // per == tp))
-        def _():
-            gots[turn][0, lax.rem(block, per)] = parts[turn][y, block]
+        slot = lax.rem(y + r, 2)
+        parts[turn][slot, block] = jnp.dot(
+            left[slot], right, preferred_element_type=F32
+        ).astype(BF16)
+        for row, kind, used, now in cases(turn, block):
+            if row == r and now:
+                @pl.when(used)
+                def _():
+                    r_copy(turn, r, block, kind).start()
+
+        if r == 0:
+            @pl.when(both(home, block // per == tp))
+            def _():
+                gots[turn][0, lax.rem(block, per)] = parts[turn][y, block]
+
+    def scatter_early(k, turn, left, weight, count):
+        for i in range(count):
+            need(k, plain_block(i))
+        for i in range(count):
+            partner_wait(k, plain_block(i))
+            project(turn, left, weight, plain_block(i), 1)
 
     def join(turn, block):
-        for r, kind, used, now in cases(block):
+        for r, kind, used, now in cases(turn, block):
             if not now:
                 @pl.when(used)
                 def _():
@@ -793,35 +824,55 @@
         landed(turn, 2, at)
         got = gots[turn]
         total = got[0, at].astype(F32) + got[1, at].astype(F32) + got[2, at].astype(F32)
-        cols = pl.ds(pl.multiple_of(at * width, 128), width)
+        if STRAIGHT[turn]:
+            once = straight(turn, block)
+
+            @pl.when(once)
+            def _():
+                landed(turn, 3, at)
+                extra[...] = got[3, at].astype(F32)
+
+            @pl.when(jnp.logical_not(once))
+            def _():
+                extra[...] = jnp.zeros_like(extra)
+
+            total += extra[...]
         if turn == 0:
-            mid[at] = (tok[:, cols].astype(F32) + total).astype(BF16)
+            mid[at] = (tok[at].astype(F32) + total).astype(BF16)
             ag_send(1, at)
         else:
-            out[:, cols] = (mid[at].astype(F32) + total).astype(BF16)
-
-    def scatter_loop(k, turn, left, weight, beside):
+            out[at] = (mid[at].astype(F32) + total).astype(BF16)
+            out_store(at).start()
+
+    def scatter_loop(k, turn, left, weight, early, lags, beside):
+        join_lag, collect_lag = lags
+
         def step(i, _):
+            @pl.when(both(i >= early, i < n))
+            def _():
+                need(k, plain_block(i))
+
+            @pl.when(both(i >= join_lag, i < n + join_lag))
+            def _():
+                join(turn, plain_block(i - join_lag))
+
             @pl.when(i < n)
             def _():
-                need(k, plain_block(i))
-
-            @pl.when(both(i >= 1, i < n + 1))
-            def _():
-                block = plain_block(i - 1)
-                partner_wait(k, block)
-                project(turn, left, weight, block)
-
-            @pl.when(both(i >= 3, i < n + 3))
-            def _():
-                join(turn, plain_block(i - 3))
+                block = plain_block(i)
+
+                @pl.when(i >= early)
+                def _():
+                    partner_wait(k, block)
+                    project(turn, left, weight, block, 1)
+
+                project(turn, left, weight, block, 0)
 
             for at, action in beside:
                 pl.when(i == at)(action)
 
-            @pl.when(i >= 5)
-            def _():
-                block = plain_block(i - 5)
+            @pl.when(i >= collect_lag)
+            def _():
+                block = plain_block(i - collect_lag)
 
                 @pl.when(block // per == tp)
                 def _():
@@ -829,12 +880,18 @@
 
             return 0
 
-        lax.fori_loop(0, n + 5, step, 0)
-
+        lax.fori_loop(0, n + collect_lag, step, 0)
+
+    gain_loads = [
+        pltpu.make_async_copy(mix_gain_hbm, mix_gain, n_sem.at[0]),
+        pltpu.make_async_copy(ffn_gain_hbm, ffn_gain, n_sem.at[1]),
+    ]
+    for i in range(per):
+        tok_load(i).start()
     for k in range(4):
         for copy in own_load(k):
             copy.start()
-    for copy in small_local:
+    for copy in small_local + gain_loads:
         copy.start()
     for target in greeted:
         pl.semaphore_signal(barrier, inc=1, device_id=target, device_id_type=MESH)
@@ -843,10 +900,12 @@
     for copy in across(0, fs):
         copy.start()
     for i in range(per):
+        tok_load(i).wait()
         ag_send(0, i)
-    for copy in own_load(0):
-        copy.wait()
-    spread(0, fs)
+    for k in range(2):
+        for copy in own_load(k):
+            copy.wait()
+        spread(k, fs)
     for copy in across(1, fs) + small_away:
         copy.start()
     uv[...] = jnp.zeros_like(uv)
@@ -854,9 +913,11 @@
     squares[...] = jnp.zeros_like(squares)
     row_scale[...] = jnp.zeros_like(row_scale)
     cross_over(0)
-    for k in range(1, 4):
+    for k in range(2, 4):
         for copy in own_load(k):
             copy.wait()
+    for copy in gain_loads:
+        copy.wait()
     turns = [(far, at) for far in range(1, nz - 1) for at in (y, 1 - y)]
     for i in range(max(per, len(turns))):
         if i < len(turns):
@@ -864,7 +925,6 @@
         if i < per:
             for half in range(nt):
                 ag_forward(0, half * per + i)
-    spread(1, fs)
     cross_over(1)
     for k in (2, 3):
         for copy in across(k, fs):
@@ -873,8 +933,8 @@
     def in_block(cols, half):
         uv[half] += jnp.dot(normed[:, cols], g_in[half, cols], preferred_element_type=F32)
 
-    gathered_loop(0, 0, mix_gain, in_block, 0, ())
-    relay_from(1, 1, 2)
+    hops = ((nz // 2, lambda: relay(1, 1, 0)), (nz // 2 + 1, lambda: relay(1, 1, 1)))
+    gathered_loop(0, 0, mix_gain, in_block, 0, hops)
 
     for copy in small_local:
         copy.wait()
@@ -928,22 +988,28 @@
 
         lax.fori_loop(0, seq // block_len, mix_rows, 0)
 
+    def start_both(k):
+        @pl.when(y == 0)
+        def _():
+            spread(k, fs)
+            cross_over(k)
+
+        @pl.when(y == 1)
+        def _():
+            cross_over(k)
+            spread(k, fs)
+
     relay_from(1, 2, nz - 1)
-    spread(2, fs)
-    cross_over(2)
+    start_both(2)
     squares[...] = jnp.zeros_like(squares)
 
-    def start_down():
-        spread(3, fs)
-        cross_over(3)
-
     hops = (
-        (n // 2 + 1, lambda: relay(2, 1, y)),
-        (n // 2 + 2, lambda: relay(2, 1, 1 - y)),
-        (n, lambda: relay_from(2, 2, nz - 1)),
-        (n + 3, start_down),
+        (n // 2 + 2, lambda: relay(2, 1, 0)),
+        (n, lambda: relay(2, 1, 1)),
+        (n + 4, lambda: relay_from(2, 2, nz - 1)),
+        (n + 5, lambda: start_both(3)),
     )
-    scatter_loop(1, 0, hidden, g_out, hops)
+    scatter_loop(1, 0, hidden, g_out, 0, (3, 6), hops)
 
     def up_block(cols, half):
         product = jnp.dot(normed[:, cols], g_up[half, cols], preferred_element_type=F32)
@@ -954,7 +1020,8 @@
 
     taps_len = tg.shape[1]
     chunk = 128
-    for slot in range(2):
+
+    def convolve(slot):
         for half in range(nt):
             for at in range(0, cf, chunk):
                 gate = jnp.zeros((seq, chunk), F32)
@@ -973,9 +1040,14 @@
                     jax.nn.gelu(gate) * value
                 ).astype(BF16)
 
+    convolve(1 - y)
+    scatter_early(3, 1, act, g_dn, ny)
+    convolve(y)
     relay_from(3, 2, nz - 1)
-    scatter_loop(3, 1, act, g_dn, ())
-
+    scatter_loop(3, 1, act, g_dn, ny, (2, 4), ())
+
+    for i in range(per):
+        out_store(i).wait()
     for k in range(4):
         for copy in across(k, fs):
             copy.wait_send()
@@ -986,7 +1058,7 @@
         for k in range(4):
             d_copy(k, block).wait_send()
         for turn in range(2):
-            for r, kind, used, _now in cases(block):
+            for r, kind, used, _now in cases(turn, block):
                 @pl.when(used)
                 def _():
                     r_copy(turn, r, block, kind).wait_send()
@@ -1053,15 +1125,15 @@
     taps_len = taps_gate.shape[0]
     vmem, sem, hbm = pltpu.VMEM, pltpu.SemaphoreType.DMA, pl.ANY
     operands = (
-        (tokens, vmem),
-        (mix_gain[None, :], vmem),
+        (tokens, hbm),
+        (mix_gain[None, :], hbm),
         (w_u, hbm),
         (w_v, hbm),
         (norm_gain[None, :], hbm),
         (mix_weight, hbm),
         (mix_bias, hbm),
         (w_mix_out, hbm),
-        (ffn_gain[None, :], vmem),
+        (ffn_gain[None, :], hbm),
         (w_gate, hbm),
         (w_value, hbm),
         (taps_gate, hbm),
@@ -1072,8 +1144,12 @@
         functools.partial(plane_kernel, n, nr, nt),
         out_shape=jax.ShapeDtypeStruct((seq, own_width), BF16),
         in_specs=[pl.BlockSpec(memory_space=space) for _, space in operands],
-        out_specs=pl.BlockSpec(memory_space=vmem),
+        out_specs=pl.BlockSpec(memory_space=hbm),
         scratch_shapes=[
+            vmem((per, seq, width), BF16),
+            vmem((per, seq, width), BF16),
+            vmem((1, n * width), F32),
+            vmem((1, n * width), F32),
             vmem((nt, n * depth, 2 * cu), BF16),
             vmem((n, nt, cu, width), BF16),
             vmem((nt, n * depth, 2 * cf), BF16),
@@ -1088,12 +1164,13 @@
             vmem((2, seq, nt * cf), BF16),
             vmem((2, seq + 8, 1), F32),
             vmem((2, seq, 128), F32),
+            vmem((seq, width), F32),
             vmem((2, n, seq, width), BF16),
             vmem((2, n, seq, width), BF16),
             vmem((n, seq, width), BF16),
             vmem((n, seq, width), BF16),
-            vmem((3, per, seq, width), BF16),
-            vmem((3, per, seq, width), BF16),
+            vmem((4, per, seq, width), BF16),
+            vmem((4, per, seq, width), BF16),
             vmem((nt, groups // share, block_len, block_len), BF16),
             vmem((nt, groups // share, block_len, block_len), BF16),
             vmem((nt, 1, cu), F32),
@@ -1101,6 +1178,9 @@
             vmem((nt, groups // share, block_len, 1), F32),
             vmem((nt, taps_len, cf), BF16),
             vmem((nt, taps_len, cf), BF16),
+            sem((per,)),
+            sem((per,)),
+            sem((2,)),
             sem((4, 2)),
             sem((4, 2)),
             sem((4, 2)),
@@ -1116,7 +1196,7 @@
             sem((2, n)),
             sem((2, 2, n)),
             sem((2, n)),
-            sem((2, 3, per)),
+            sem((2, 4, per)),
         ],
         compiler_params=pltpu.CompilerParams(
             collective_id=0, has_side_effects=True, vmem_limit_bytes=67043328

time: 157 us -> 152 us (0.968)
  Pallas kernels: 155 us -> 149 us
    pallas_call x1, Pallas kernels: 155 us -> 149 us  [on_plane(): pl.pallas_call(functools.partial(plane_kernel, n, nr, nt), out_shape=jax....]
where the time goes in v4:
time: 152 us; the launch traced here: 151 us
  Pallas kernels  149 us (98%)
  local copies, waits for them, and re-layouts  2.06 us (1%)
    pallas_call x1, Pallas kernels, on_plane(): pl.pallas_call(functools.partial(plane_kernel, n, nr, nt), out_shape=jax....  149 us

profile of v4, /device:TPU:1, one launch (start us, length us, event | category | flops | bytes accessed | tf_op | source)
XLA Modules:
  0.0 151.1 jit_solution(10355189769462157075)
XLA Ops:
  0.0 149.0 %shard_map.136 = bf16[384,1024]{1,0:T(8,128)(2,1)} custom-call(bf16[384,1024]{1,0:T(8,128)(2,1)} %tok_hbm.1, f32[1,2048]{1,0:T(1,128)} %bitcast.3, bf16[256,1024]{1,0:T(8,128)(2,1)} %w_u.1, bf16[256,1024]{1,0:T(8,128)(2,1)} %w_v.1, f32[1,1024]{1,0:T(1,128)} %bitcast.5, bf16[8,128,128]{2,1,0:T(8,128)(2,1)} %mixw.1, f32[8,128]{1,0:T(8,128)} %bias.1, ...), custom_call_target="tpu_custom_call" | custom-call | tf_op jit(solution)/shard_map/pallas_call | solution.py:1143
  149.0 2.1 %copy.16 = bf16[384,1024]{1,0:T(8,128)(2,1)} copy(bf16[384,1024]{1,0:T(8,128)(2,1)} %shard_map.136) | data formatting | bytes 1572864

commit v5 on v4

--- a/solution.py
+++ b/solution.py
@@ -441,7 +441,7 @@
     away = rep != tp
     cu, cf = g_out.shape[2], g_dn.shape[2]
     depth = w_u.shape[0]
-    few = (max(1, per // 4), max(1, per // 2))
+    few = (max(1, per // 4), max(1, per // 4))
     feats = (feat, feat2)
 
     def both(*conditions):

time: 152 us -> 151 us (level)
  no operation moved by 1% of the time
where the time goes in v5:
time: 151 us
  Pallas kernels  149 us (99%)
  local copies, waits for them, and re-layouts  2.06 us (1%)
    pallas_call x1, Pallas kernels, on_plane(): pl.pallas_call(functools.partial(plane_kernel, n, nr, nt), out_shape=jax....  149 us

profile of v5, /device:TPU:1, one launch (start us, length us, event | category | flops | bytes accessed | tf_op | source)
XLA Modules:
  0.0 151.1 jit_solution(15965993547091430364)
XLA Ops:
  0.0 149.0 %shard_map.136 = bf16[384,1024]{1,0:T(8,128)(2,1)} custom-call(bf16[384,1024]{1,0:T(8,128)(2,1)} %tok_hbm.1, f32[1,2048]{1,0:T(1,128)} %bitcast.3, bf16[256,1024]{1,0:T(8,128)(2,1)} %w_u.1, bf16[256,1024]{1,0:T(8,128)(2,1)} %w_v.1, f32[1,1024]{1,0:T(1,128)} %bitcast.5, bf16[8,128,128]{2,1,0:T(8,128)(2,1)} %mixw.1, f32[8,128]{1,0:T(8,128)} %bias.1, ...), custom_call_target="tpu_custom_call" | custom-call | tf_op jit(solution)/shard_map/pallas_call | solution.py:1143
  149.0 2.1 %copy.16 = bf16[384,1024]{1,0:T(8,128)(2,1)} copy(bf16[384,1024]{1,0:T(8,128)(2,1)} %shard_map.136) | data formatting | bytes 1572864
